TPU v7x, 32 devices: a whole 2x2x4 slice. The times are simulated.
32 devices in a mesh: sp: 8 (over z, y), tp: 4 (over x, core).
Axes of the slice: x: 2, y: 2, z: 4, core: 2. Of those that a mesh axis runs over, the one named last changes fastest.
Arguments:
- stream: bfloat16 [3072, 2048], P(('sp', 'tp')), may hold values from -6 to 6
- query_projected: bfloat16 [3072, 1024], P('sp', 'tp'), may hold values from -6 to 6
- key_projected: bfloat16 [3072, 1024], P('sp', 'tp'), may hold values from -6 to 6
- value_projected: bfloat16 [3072, 1024], P('sp', 'tp'), may hold values from -6 to 6
- gate_projected: bfloat16 [3072, 1024], P('sp', 'tp'), may hold values from -6 to 6
- strength_logits: bfloat16 [8, 3072], P('tp', 'sp'), may hold values from -7 to 4
- decay_preactivation: bfloat16 [8, 3072], P('tp', 'sp'), may hold values from -9 to 9
- extra_log_decay: float32 [8, 3072], P('tp', 'sp'), may hold values from -0.7 to 0
- head_decay_rate: float32 [8], P('tp'), may hold values from 0 to 0.1
- head_norm_gain: float32 [128], replicated, may hold values from 0.1 to 1.9
- head_output_matrix: bfloat16 [1024, 2048], P('tp'), may hold values from -0.1875 to 0.1875
- feed_norm_gain: float32 [2048], replicated, may hold values from 0.1 to 1.9
- gate_matrix: bfloat16 [2048, 5632], P('sp', 'tp'), may hold values from -0.125 to 0.125
- up_matrix: bfloat16 [2048, 5632], P('sp', 'tp'), may hold values from -0.125 to 0.125
- down_matrix: bfloat16 [5632, 2048], P('tp', 'sp'), may hold values from -0.078125 to 0.078125
Outputs:
- result: bfloat16 [3072, 2048], P(('sp', 'tp'))
All inputs are finite; a program needn't handle non-finite values.
Results may differ from a plain program's by a relative error of at most 0.015.
Values may be sent and summed in bfloat16 or wider, within the bound.
A program may use at most 128 MiB of HBM per device.

v0:
```python
import functools

import jax
import jax.numpy as jnp
from jax import lax
from jax.experimental import pallas as pl
from jax.experimental.pallas import tpu as pltpu
from jax.sharding import PartitionSpec as P

HEAD = 128
CHUNK = 128
EPSILON = 1e-06
F32 = jnp.float32
BF16 = jnp.bfloat16
HIGHEST = lax.Precision.HIGHEST
NN = (((1,), (0,)), ((), ()))
NT = (((1,), (1,)), ((), ()))
TN = (((0,), (0,)), ((), ()))


def dot1(a, b, dims=NN):
    return lax.dot_general(a, b, dims, preferred_element_type=F32)


def halves(x):
    high = x.astype(BF16)
    return high, (x - high.astype(F32)).astype(BF16)


def dot3(a, b, dims=NN):
    ah, al = halves(a)
    bh, bl = halves(b)
    return dot1(ah, bh, dims) + (dot1(ah, bl, dims) + dot1(al, bh, dims))


def silu(x):
    return x * jax.nn.sigmoid(x)


def messages(ring):
    own_z = [(a, 0, 0, way) for a in "GU" for way in "RL"]
    own_y = [(a, 0, 0, "Y") for a in "GU"]
    first = own_z + own_y
    down_y = [("D", 0, 0, "Y")]

    def relay(a, j, skip_y=False):
        out = []
        if j < ring - 1:
            out += [(a, -j, 0, "R"), (a, j, 0, "L")]
        if not skip_y:
            out += [(a, -j, 0, "Y"), (a, j, 0, "Y")]
        return out

    early, middle, later, last = [], [], [], []
    if ring > 1:
        early = relay("G", 1)
        middle = relay("U", 1)
        for j in range(2, ring):
            later += relay("G", j) + relay("U", j)
            if j == 2:
                later += [("D", 0, 0, "R"), ("D", 0, 0, "L")]
        if ring == 2:
            later += [("D", 0, 0, "R"), ("D", 0, 0, "L")]
        later += [("D", 0, 1, "R"), ("D", 0, 1, "L")]
        later += relay("D", 1, skip_y=True)
        for j in range(2, ring):
            last += relay("D", j)
    else:
        first = own_y
    return first, down_y, early, middle, later, last


def kernel(
    n, tps, groups,
    stream, qp, kp, vp, gp, strength, decay_pre, extra, rate, head_gain, w_out, feed_gain,
    gate_in, up_in, down_in,
    result,
    gate_all, up_all, down_all, out_scr, x_send, x_part, p_send, p_recv, s_in, mixed,
    d_send, d_recv, residual, rows_all, hidden, f_part, f_recv,
    w_send, w_recv, own_sem, x_sem, p_ssem, p_rsem, d_ssem, d_rsem, e_ssem, e_rsem, f_ssem, f_rsem,
):
    ring = n // 2
    sp = lax.axis_index("sp")
    tp = lax.axis_index("tp")
    r = sp // 2
    p = lax.rem(sp, 2)
    heads = strength.shape[0]
    tokens = strength.shape[1]
    chunks = tokens // CHUNK
    own_rows = stream.shape[0]
    kr = gate_in.shape[0]
    MESH = pl.DeviceIdType.MESH

    def sp_of(dr, rel):
        q = p if rel == 0 else 1 - p
        return lax.rem(r + dr + ring, ring) * 2 + q

    partner = sp_of(0, 1)
    where = {"R": sp_of(1, 0), "L": sp_of(-1, 0), "Y": partner}

    def tp_peer(o):
        return lax.rem(tp + o, tps)

    barrier = pltpu.get_barrier_semaphore()
    for dr in range(1, ring):
        pl.semaphore_signal(barrier, 1, device_id=(sp_of(dr, 0), tp), device_id_type=MESH)
    pl.semaphore_signal(barrier, 1, device_id=(partner, tp), device_id_type=MESH)
    for o in range(1, tps):
        pl.semaphore_signal(barrier, 1, device_id=(sp, tp_peer(o)), device_id_type=MESH)
    pl.semaphore_wait(barrier, ring + tps - 1)

    flat = [m for g in groups for m in g]
    number = {m: i for i, m in enumerate(flat)}
    arrival = {}
    for (a, dr, rel, way) in flat:
        to = {"R": (dr - 1, rel), "L": (dr + 1, rel), "Y": (dr, 1 - rel)}[way]
        key = (a, to[0], to[1])
        assert key not in arrival
        arrival[key] = number[(a, dr, rel, way)]
    waited = set()
    copies = []

    def exists(dr):
        return (r + dr >= 0) & (r + dr < ring)

    def slot(a, dr, rel):
        s = sp_of(dr, rel)
        if a == "D":
            return down_all.at[s]
        whole = gate_all if a == "G" else up_all
        return whole.at[pl.ds(pl.multiple_of(s * kr, kr), kr), :]

    inputs = {"G": gate_in, "U": up_in, "D": down_in}

    def need(a, dr, rel):
        key = (a, dr, rel)
        if (dr == 0 and rel == 0) or key in waited:
            return
        waited.add(key)
        m = arrival[key]

        @pl.when(exists(dr))
        def _():
            here = slot(*key)
            pltpu.make_async_remote_copy(
                here, here, w_send.at[m], w_recv.at[m], device_id=(partner, tp), device_id_type=MESH
            ).wait_recv()

    def outgoing(message):
        a, dr, rel, way = message
        m = number[message]
        return pltpu.make_async_remote_copy(
            inputs[a] if dr == 0 and rel == 0 else slot(a, dr, rel),
            slot(a, dr, rel),
            w_send.at[m], w_recv.at[m],
            device_id=(where[way], tp), device_id_type=MESH,
        )

    def goes(message):
        ahead = {"R": r + 1 < ring, "L": r >= 1, "Y": r >= 0}[message[3]]
        return exists(message[1]) & ahead

    def pump(group):
        for message in group:
            need(*message[:3])

            @pl.when(goes(message))
            def _():
                outgoing(message).start()

            copies.append(message)

    def need_all(a):
        for dr in sorted(range(1 - ring, ring), key=abs):
            for rel in (0, 1):
                need(a, dr, rel)

    first, down_y, early, middle, later, last_group = groups
    pump(first)
    locals_ = []
    for i, a in enumerate("GUD"):
        local = pltpu.make_async_copy(inputs[a], slot(a, 0, 0), own_sem.at[i])
        local.start()
        locals_.append(local)

    row_i = lax.broadcasted_iota(jnp.int32, (CHUNK, CHUNK), 0)
    col_i = lax.broadcasted_iota(jnp.int32, (CHUNK, CHUNK), 1)
    causal = row_i >= col_i
    strict = row_i > col_i
    eye = jnp.where(row_i == col_i, 1.0, 0.0).astype(F32)
    lower = jnp.where(causal, 1.0, 0.0).astype(F32)
    beta = jax.nn.sigmoid(strength[...].astype(F32))
    pre = decay_pre[...].astype(F32)
    soft = jnp.maximum(pre, 0.0) + jnp.log1p(jnp.exp(-jnp.abs(pre)))
    log_decay = -rate[...] * soft + extra[...]

    pairs = [(h, c) for c in range(chunks) for h in range(heads)]
    data = {}
    for c in range(chunks):
        span = slice(c * CHUNK, (c + 1) * CHUNK)
        ld = log_decay[:, span]
        c_row = lax.dot_general(ld, lower, NT, precision=HIGHEST, preferred_element_type=F32)
        c_col = lax.dot_general(lower, ld, NT, precision=HIGHEST, preferred_element_type=F32)
        b_col = lax.dot_general(eye, beta[:, span], NT, precision=HIGHEST, preferred_element_type=F32)
        for h in range(heads):
            lanes = slice(h * HEAD, (h + 1) * HEAD)
            q = qp[span, lanes].astype(F32)
            k = kp[span, lanes].astype(F32)
            v = vp[span, lanes].astype(F32)
            q = q * (lax.rsqrt(jnp.sum(q * q, axis=-1, keepdims=True) + EPSILON) * HEAD ** (-0.5))
            k = k * lax.rsqrt(jnp.sum(k * k, axis=-1, keepdims=True) + EPSILON)
            cc = c_col[:, h:h + 1]
            bb = b_col[:, h:h + 1]
            cr = c_row[h:h + 1, :]
            last = cr[:, CHUNK - 1:]
            damp = jnp.where(causal, jnp.exp(jnp.where(causal, cc - cr, 0.0)), 0.0)
            grown = jnp.exp(cc)
            kb = k * bb
            kk = dot3(kb, k, NT) * jnp.where(strict, damp, 0.0)
            inner = dot3(q, k, NT) * damp
            data[h, c] = dict(
                low=kk, inner=inner, v=v * bb, kw=kb * grown, qd=q * grown,
                kd=k * jnp.exp(last - cc), decay=jnp.exp(last),
            )
    inverse = {}
    b = 1
    shift = 0
    while b < CHUNK:
        mask = ((row_i >> (shift + 1)) == (col_i >> (shift + 1))) & (
            ((row_i >> shift) & 1) == 1) & (((col_i >> shift) & 1) == 0)
        for key in pairs:
            piece = jnp.where(mask, data[key]["low"], 0.0)
            if b == 1:
                inverse[key] = eye - piece
            else:
                x = inverse[key]
                inverse[key] = x - dot3(x, dot3(piece, x))
        b *= 2
        shift += 1
    states = [jnp.concatenate([jnp.zeros((HEAD, HEAD), F32), eye], axis=1) for _ in range(heads)]
    for c in range(chunks):
        for h in range(heads):
            e = data[h, c]
            u = dot3(inverse[h, c], e["v"])
            w = dot3(inverse[h, c], e["kw"])
            x = states[h]
            new = jnp.concatenate([u, jnp.zeros_like(u)], axis=1) - dot3(w, x)
            out_scr[h, c * CHUNK:(c + 1) * CHUNK, :] = dot3(e["qd"], x) + dot3(e["inner"], new)
            states[h] = e["decay"] * x + dot3(e["kd"], new, TN)

    for h in range(heads):
        x_send[h] = states[h].astype(BF16)
    x_copy = pltpu.make_async_remote_copy(
        x_send, x_part, x_sem.at[0], x_sem.at[1], device_id=(partner, tp), device_id_type=MESH)
    x_copy.start()
    pump(down_y)
    x_copy.wait_recv()
    for h in range(heads):
        mine = states[h]
        theirs = x_part[h].astype(F32)
        before = jnp.where(p == 0, mine, theirs)
        after = jnp.where(p == 0, theirs, mine)
        after_s = jnp.concatenate([after[:, :HEAD], jnp.zeros((HEAD, HEAD), F32)], axis=1)
        p_send[h] = (dot3(after[:, HEAD:], before) + after_s).astype(BF16)

    def p_copy(k, to, at):
        return pltpu.make_async_remote_copy(
            p_send, p_recv.at[at], p_ssem.at[k], p_rsem.at[k],
            device_id=(to, tp), device_id_type=MESH)

    for k in range(1, ring):
        @pl.when(r + k < ring)
        def _():
            p_copy(k, sp_of(k, 0), r).start()
    pump(early)
    for k in range(1, ring):
        @pl.when(r - k >= 0)
        def _():
            p_copy(k, sp_of(-k, 0), r - k).wait_recv()
    s_in[...] = jnp.zeros_like(s_in)

    def fold(i, _):
        for h in range(heads):
            got = p_recv[i, h].astype(F32)
            s_in[h] = dot3(got[:, HEAD:], s_in[h]) + got[:, :HEAD]
        return 0

    lax.fori_loop(0, r, fold, 0)
    for h in range(heads):
        lanes = slice(h * HEAD, (h + 1) * HEAD)
        got = x_part[h].astype(F32)
        s = s_in[h]
        s = jnp.where(p == 0, s, dot3(got[:, HEAD:], s) + got[:, :HEAD])
        att = out_scr[h, :, :HEAD] + dot3(out_scr[h, :, HEAD:], s)
        att = att * lax.rsqrt(jnp.mean(att * att, axis=-1, keepdims=True) + EPSILON) * head_gain[...]
        mixed[:, lanes] = (att * silu(gp[:, lanes].astype(F32))).astype(BF16)

    def rows_of(t):
        return pl.ds(pl.multiple_of(t * own_rows, own_rows), own_rows)

    order = [o for o in (2, 3, 1) if o < tps] + list(range(4, tps))
    d_copies = []
    for o in order:
        to = tp_peer(o)
        d_send[o - 1] = dot1(mixed[rows_of(to), :], w_out[...]).astype(BF16)
        copy = pltpu.make_async_remote_copy(
            d_send.at[o - 1], d_recv.at[o - 1], d_ssem.at[o - 1], d_rsem.at[o - 1],
            device_id=(sp, to), device_id_type=MESH)
        copy.start()
        d_copies.append(copy)
    pump(middle)
    total = dot1(mixed[rows_of(tp), :], w_out[...]).astype(BF16).astype(F32)
    for copy in d_copies:
        copy.wait_recv()
    for o in range(1, tps):
        total = total + d_recv[o - 1].astype(F32)
    total = stream[...].astype(F32) + total
    residual[...] = total
    rows_all[rows_of(tp), :] = (
        total * lax.rsqrt(jnp.mean(total * total, axis=-1, keepdims=True) + EPSILON) * feed_gain[...]
    ).astype(BF16)
    e_copies = []
    for o in order:
        copy = pltpu.make_async_remote_copy(
            rows_all.at[rows_of(tp), :], rows_all.at[rows_of(tp), :], e_ssem.at[o - 1], e_rsem.at[o - 1],
            device_id=(sp, tp_peer(o)), device_id_type=MESH)
        copy.start()
        e_copies.append(copy)
    for o in order:
        there = rows_all.at[rows_of(lax.rem(tp - o + tps, tps)), :]
        pltpu.make_async_remote_copy(
            there, there, e_ssem.at[o - 1], e_rsem.at[o - 1],
            device_id=(sp, tp_peer(o)), device_id_type=MESH).wait_recv()
    pump(later)
    need_all("G")
    need_all("U")
    for local in locals_:
        local.wait()

    tile = 128

    def ffn_in(i, _):
        lanes = pl.ds(pl.multiple_of(i * tile, tile), tile)
        both = dot1(rows_all[...], jnp.concatenate([gate_all[:, lanes], up_all[:, lanes]], axis=1))
        hidden[:, lanes] = (silu(both[:, :tile]) * both[:, tile:]).astype(BF16)
        return 0

    lax.fori_loop(0, gate_all.shape[1] // tile, ffn_in, 0)
    pump(last_group)
    need_all("D")
    dc = down_all.shape[2]
    pack = max(1, 128 // dc)
    wide = pack * dc

    def ffn_out(i, _):
        lanes = pl.ds(pl.multiple_of(i * wide, wide), wide)
        if pack == 1:
            weights = down_all[i]
        else:
            weights = jnp.concatenate([down_all[i * pack + j] for j in range(pack)], axis=1)
        f_part[:, lanes] = dot1(hidden[...], weights).astype(BF16)
        return 0

    lax.fori_loop(0, n // pack, ffn_out, 0)
    f_copies = []
    for o in order:
        copy = pltpu.make_async_remote_copy(
            f_part.at[rows_of(tp_peer(o)), :], f_recv.at[o - 1], f_ssem.at[o - 1], f_rsem.at[o - 1],
            device_id=(sp, tp_peer(o)), device_id_type=MESH)
        copy.start()
        f_copies.append(copy)
    ffn = f_part[rows_of(tp), :].astype(F32)
    for copy in f_copies:
        copy.wait_recv()
    for o in range(1, tps):
        ffn = ffn + f_recv[o - 1].astype(F32)
    result[...] = (residual[...] + ffn).astype(BF16)

    for message in copies:
        @pl.when(goes(message))
        def _():
            outgoing(message).wait_send()
    for copy in [x_copy] + d_copies + e_copies + f_copies:
        copy.wait_send()
    for k in range(1, ring):
        @pl.when(r + k < ring)
        def _():
            p_copy(k, sp_of(k, 0), r).wait_send()


def body(n, tps, stream, qp, kp, vp, gp, strength, decay_pre, extra, rate, head_gain, w_out,
         feed_gain, gate_m, up_m, down_m):
    heads, tokens = strength.shape
    own, width = stream.shape
    kr, units = gate_m.shape
    ring = n // 2
    groups = messages(ring)
    count = sum(len(g) for g in groups)
    dma = pltpu.SemaphoreType.DMA
    vmem = pl.BlockSpec(memory_space=pltpu.VMEM)
    hbm = pl.BlockSpec(memory_space=pl.ANY)
    peers = max(1, tps - 1)
    return pl.pallas_call(
        functools.partial(kernel, n, tps, groups),
        out_shape=jax.ShapeDtypeStruct((own, width), BF16),
        in_specs=[vmem] * 12 + [hbm] * 3,
        out_specs=vmem,
        scratch_shapes=[
            pltpu.VMEM((kr * n, units), BF16),
            pltpu.VMEM((kr * n, units), BF16),
            pltpu.VMEM((n,) + down_m.shape, BF16),
            pltpu.VMEM((heads, tokens, 2 * HEAD), F32),
            pltpu.VMEM((heads, HEAD, 2 * HEAD), BF16),
            pltpu.VMEM((heads, HEAD, 2 * HEAD), BF16),
            pltpu.VMEM((heads, HEAD, 2 * HEAD), BF16),
            pltpu.VMEM((ring, heads, HEAD, 2 * HEAD), BF16),
            pltpu.VMEM((heads, HEAD, HEAD), F32),
            pltpu.VMEM((tokens, heads * HEAD), BF16),
            pltpu.VMEM((peers, own, width), BF16),
            pltpu.VMEM((peers, own, width), BF16),
            pltpu.VMEM((own, width), F32),
            pltpu.VMEM((tokens, width), BF16),
            pltpu.VMEM((tokens, units), BF16),
            pltpu.VMEM((tokens, width), BF16),
            pltpu.VMEM((peers, own, width), BF16),
            dma((count,)), dma((count,)), dma((3,)), dma((2,)), dma((ring,)), dma((ring,)),
            dma((peers,)), dma((peers,)), dma((peers,)), dma((peers,)), dma((peers,)), dma((peers,)),
        ],
        compiler_params=pltpu.CompilerParams(
            collective_id=0, has_side_effects=True, vmem_limit_bytes=60 * 1024 * 1024),
    )(stream, qp, kp, vp, gp, strength, decay_pre, extra, rate[:, None], head_gain[None, :], w_out,
      feed_gain[None, :], gate_m, up_m, down_m)


def solution(mesh):
    placed = (
        P(("sp", "tp"), None),
        P("sp", "tp"),
        P("sp", "tp"),
        P("sp", "tp"),
        P("sp", "tp"),
        P("tp", "sp"),
        P("tp", "sp"),
        P("tp", "sp"),
        P("tp"),
        P(),
        P("tp", None),
        P(),
        P("sp", "tp"),
        P("sp", "tp"),
        P("tp", "sp"),
    )
    return jax.shard_map(
        functools.partial(body, mesh.shape["sp"], mesh.shape["tp"]),
        mesh=mesh, in_specs=placed, out_specs=P(("sp", "tp"), None), check_vma=False,
    )
```

profile of v0, /device:TPU:0, one launch (start us, length us, event | category | flops | bytes accessed | tf_op | source)
XLA Modules:
  0.0 213.5 jit_solution(2801789167626529858)
XLA Ops:
  0.0 0.0 copy-start
  0.0 0.7 copy-done
  0.7 0.6 copy.16.rate
  1.3 210.4 %shard_map.145 = bf16[96,2048]{1,0:T(8,128)(2,1)} custom-call(bf16[96,2048]{1,0:T(8,128)(2,1)} %stream.1, bf16[384,256]{1,0:T(8,128)(2,1)} %qp.1, bf16[384,256]{1,0:T(8,128)(2,1)} %kp.1, bf16[384,256]{1,0:T(8,128)(2,1)} %vp.1, bf16[384,256]{1,0:T(8,128)(2,1)} %gp.1, bf16[2,384]{1,0:T(2,128)(2,1)} %strength.1, bf16[2,384]{1,0:T(2,128)(2,1)} %decay_pre.1, ...), custom_call_target="tpu_custom_call" | custom-call | tf_op jit(solution)/shard_map/pallas_call | solution.py:403
  211.7 1.8 copy.18
Async XLA Ops:
  0.0 0.7 copy-start
where the time goes:
time: 214 us; the launch traced here: 213 us
  Pallas kernels  210 us (98%)
  local copies, waits for them, and re-layouts  3.07 us (1%)
    pallas_call x1, Pallas kernels, body(): pl.pallas_call(functools.partial(kernel, n, tps, groups), out_shape=jax.S...  210 us

commit v1 on v0

--- a/solution.py
+++ b/solution.py
@@ -9,6 +9,7 @@
 
 HEAD = 128
 CHUNK = 128
+UNROLLED = 8
 EPSILON = 1e-06
 F32 = jnp.float32
 BF16 = jnp.bfloat16
@@ -37,152 +38,9 @@
     return x * jax.nn.sigmoid(x)
 
 
-def messages(ring):
-    own_z = [(a, 0, 0, way) for a in "GU" for way in "RL"]
-    own_y = [(a, 0, 0, "Y") for a in "GU"]
-    first = own_z + own_y
-    down_y = [("D", 0, 0, "Y")]
-
-    def relay(a, j, skip_y=False):
-        out = []
-        if j < ring - 1:
-            out += [(a, -j, 0, "R"), (a, j, 0, "L")]
-        if not skip_y:
-            out += [(a, -j, 0, "Y"), (a, j, 0, "Y")]
-        return out
-
-    early, middle, later, last = [], [], [], []
-    if ring > 1:
-        early = relay("G", 1)
-        middle = relay("U", 1)
-        for j in range(2, ring):
-            later += relay("G", j) + relay("U", j)
-            if j == 2:
-                later += [("D", 0, 0, "R"), ("D", 0, 0, "L")]
-        if ring == 2:
-            later += [("D", 0, 0, "R"), ("D", 0, 0, "L")]
-        later += [("D", 0, 1, "R"), ("D", 0, 1, "L")]
-        later += relay("D", 1, skip_y=True)
-        for j in range(2, ring):
-            last += relay("D", j)
-    else:
-        first = own_y
-    return first, down_y, early, middle, later, last
-
-
-def kernel(
-    n, tps, groups,
-    stream, qp, kp, vp, gp, strength, decay_pre, extra, rate, head_gain, w_out, feed_gain,
-    gate_in, up_in, down_in,
-    result,
-    gate_all, up_all, down_all, out_scr, x_send, x_part, p_send, p_recv, s_in, mixed,
-    d_send, d_recv, residual, rows_all, hidden, f_part, f_recv,
-    w_send, w_recv, own_sem, x_sem, p_ssem, p_rsem, d_ssem, d_rsem, e_ssem, e_rsem, f_ssem, f_rsem,
-):
-    ring = n // 2
-    sp = lax.axis_index("sp")
-    tp = lax.axis_index("tp")
-    r = sp // 2
-    p = lax.rem(sp, 2)
-    heads = strength.shape[0]
-    tokens = strength.shape[1]
+def local_scan(qp, kp, vp, strength, decay_pre, extra, rate, out_scr):
+    heads, tokens = strength.shape
     chunks = tokens // CHUNK
-    own_rows = stream.shape[0]
-    kr = gate_in.shape[0]
-    MESH = pl.DeviceIdType.MESH
-
-    def sp_of(dr, rel):
-        q = p if rel == 0 else 1 - p
-        return lax.rem(r + dr + ring, ring) * 2 + q
-
-    partner = sp_of(0, 1)
-    where = {"R": sp_of(1, 0), "L": sp_of(-1, 0), "Y": partner}
-
-    def tp_peer(o):
-        return lax.rem(tp + o, tps)
-
-    barrier = pltpu.get_barrier_semaphore()
-    for dr in range(1, ring):
-        pl.semaphore_signal(barrier, 1, device_id=(sp_of(dr, 0), tp), device_id_type=MESH)
-    pl.semaphore_signal(barrier, 1, device_id=(partner, tp), device_id_type=MESH)
-    for o in range(1, tps):
-        pl.semaphore_signal(barrier, 1, device_id=(sp, tp_peer(o)), device_id_type=MESH)
-    pl.semaphore_wait(barrier, ring + tps - 1)
-
-    flat = [m for g in groups for m in g]
-    number = {m: i for i, m in enumerate(flat)}
-    arrival = {}
-    for (a, dr, rel, way) in flat:
-        to = {"R": (dr - 1, rel), "L": (dr + 1, rel), "Y": (dr, 1 - rel)}[way]
-        key = (a, to[0], to[1])
-        assert key not in arrival
-        arrival[key] = number[(a, dr, rel, way)]
-    waited = set()
-    copies = []
-
-    def exists(dr):
-        return (r + dr >= 0) & (r + dr < ring)
-
-    def slot(a, dr, rel):
-        s = sp_of(dr, rel)
-        if a == "D":
-            return down_all.at[s]
-        whole = gate_all if a == "G" else up_all
-        return whole.at[pl.ds(pl.multiple_of(s * kr, kr), kr), :]
-
-    inputs = {"G": gate_in, "U": up_in, "D": down_in}
-
-    def need(a, dr, rel):
-        key = (a, dr, rel)
-        if (dr == 0 and rel == 0) or key in waited:
-            return
-        waited.add(key)
-        m = arrival[key]
-
-        @pl.when(exists(dr))
-        def _():
-            here = slot(*key)
-            pltpu.make_async_remote_copy(
-                here, here, w_send.at[m], w_recv.at[m], device_id=(partner, tp), device_id_type=MESH
-            ).wait_recv()
-
-    def outgoing(message):
-        a, dr, rel, way = message
-        m = number[message]
-        return pltpu.make_async_remote_copy(
-            inputs[a] if dr == 0 and rel == 0 else slot(a, dr, rel),
-            slot(a, dr, rel),
-            w_send.at[m], w_recv.at[m],
-            device_id=(where[way], tp), device_id_type=MESH,
-        )
-
-    def goes(message):
-        ahead = {"R": r + 1 < ring, "L": r >= 1, "Y": r >= 0}[message[3]]
-        return exists(message[1]) & ahead
-
-    def pump(group):
-        for message in group:
-            need(*message[:3])
-
-            @pl.when(goes(message))
-            def _():
-                outgoing(message).start()
-
-            copies.append(message)
-
-    def need_all(a):
-        for dr in sorted(range(1 - ring, ring), key=abs):
-            for rel in (0, 1):
-                need(a, dr, rel)
-
-    first, down_y, early, middle, later, last_group = groups
-    pump(first)
-    locals_ = []
-    for i, a in enumerate("GUD"):
-        local = pltpu.make_async_copy(inputs[a], slot(a, 0, 0), own_sem.at[i])
-        local.start()
-        locals_.append(local)
-
     row_i = lax.broadcasted_iota(jnp.int32, (CHUNK, CHUNK), 0)
     col_i = lax.broadcasted_iota(jnp.int32, (CHUNK, CHUNK), 1)
     causal = row_i >= col_i
@@ -247,14 +105,11 @@
             new = jnp.concatenate([u, jnp.zeros_like(u)], axis=1) - dot3(w, x)
             out_scr[h, c * CHUNK:(c + 1) * CHUNK, :] = dot3(e["qd"], x) + dot3(e["inner"], new)
             states[h] = e["decay"] * x + dot3(e["kd"], new, TN)
-
-    for h in range(heads):
-        x_send[h] = states[h].astype(BF16)
-    x_copy = pltpu.make_async_remote_copy(
-        x_send, x_part, x_sem.at[0], x_sem.at[1], device_id=(partner, tp), device_id_type=MESH)
-    x_copy.start()
-    pump(down_y)
-    x_copy.wait_recv()
+    return states
+
+
+def combine(states, x_part, p, p_send):
+    heads = len(states)
     for h in range(heads):
         mine = states[h]
         theirs = x_part[h].astype(F32)
@@ -263,20 +118,8 @@
         after_s = jnp.concatenate([after[:, :HEAD], jnp.zeros((HEAD, HEAD), F32)], axis=1)
         p_send[h] = (dot3(after[:, HEAD:], before) + after_s).astype(BF16)
 
-    def p_copy(k, to, at):
-        return pltpu.make_async_remote_copy(
-            p_send, p_recv.at[at], p_ssem.at[k], p_rsem.at[k],
-            device_id=(to, tp), device_id_type=MESH)
-
-    for k in range(1, ring):
-        @pl.when(r + k < ring)
-        def _():
-            p_copy(k, sp_of(k, 0), r).start()
-    pump(early)
-    for k in range(1, ring):
-        @pl.when(r - k >= 0)
-        def _():
-            p_copy(k, sp_of(-k, 0), r - k).wait_recv()
+
+def fold_states(r, p_recv, s_in, heads):
     s_in[...] = jnp.zeros_like(s_in)
 
     def fold(i, _):
@@ -286,6 +129,9 @@
         return 0
 
     lax.fori_loop(0, r, fold, 0)
+
+
+def apply_state(p, x_part, s_in, out_scr, head_gain, gp, mixed, heads):
     for h in range(heads):
         lanes = slice(h * HEAD, (h + 1) * HEAD)
         got = x_part[h].astype(F32)
@@ -294,6 +140,180 @@
         att = out_scr[h, :, :HEAD] + dot3(out_scr[h, :, HEAD:], s)
         att = att * lax.rsqrt(jnp.mean(att * att, axis=-1, keepdims=True) + EPSILON) * head_gain[...]
         mixed[:, lanes] = (att * silu(gp[:, lanes].astype(F32))).astype(BF16)
+
+
+def messages(ring):
+    own_z = [(a, 0, 0, way) for a in "GU" for way in "RL"]
+    own_y = [(a, 0, 0, "Y") for a in "GU"]
+    first = own_z + own_y
+    down_y = [("D", 0, 0, "Y")]
+
+    def relay(a, j, skip_y=False):
+        out = []
+        if j < ring - 1:
+            out += [(a, -j, 0, "R"), (a, j, 0, "L")]
+        if not skip_y:
+            out += [(a, -j, 0, "Y"), (a, j, 0, "Y")]
+        return out
+
+    early, middle, later, last = [], [], [], []
+    if ring > 1:
+        early = relay("G", 1)
+        middle = relay("U", 1)
+        for j in range(2, ring):
+            later += relay("G", j) + relay("U", j)
+            if j == 2:
+                later += [("D", 0, 0, "R"), ("D", 0, 0, "L")]
+        if ring == 2:
+            later += [("D", 0, 0, "R"), ("D", 0, 0, "L")]
+        later += [("D", 0, 1, "R"), ("D", 0, 1, "L")]
+        later += relay("D", 1, skip_y=True)
+        for j in range(2, ring):
+            last += relay("D", j)
+    else:
+        first = own_y
+    return first, down_y, early, middle, later, last
+
+
+def chain_kernel(
+    n, tps, groups,
+    stream, qp, kp, vp, gp, strength, decay_pre, extra, rate, head_gain, w_out, feed_gain,
+    gate_in, up_in, down_in,
+    result,
+    gate_all, up_all, down_all, out_scr, x_send, x_part, p_send, p_recv, s_in, mixed,
+    d_send, d_recv, residual, rows_all, hidden, f_part, f_recv,
+    w_send, w_recv, own_sem, x_sem, p_ssem, p_rsem, d_ssem, d_rsem, e_ssem, e_rsem, f_ssem, f_rsem,
+):
+    ring = n // 2
+    sp = lax.axis_index("sp")
+    tp = lax.axis_index("tp")
+    r = sp // 2
+    p = lax.rem(sp, 2)
+    heads = strength.shape[0]
+    tokens = strength.shape[1]
+    chunks = tokens // CHUNK
+    own_rows = stream.shape[0]
+    kr = gate_in.shape[0]
+    MESH = pl.DeviceIdType.MESH
+
+    def sp_of(dr, rel):
+        q = p if rel == 0 else 1 - p
+        return lax.rem(r + dr + ring, ring) * 2 + q
+
+    partner = sp_of(0, 1)
+    where = {"R": sp_of(1, 0), "L": sp_of(-1, 0), "Y": partner}
+
+    def tp_peer(o):
+        return lax.rem(tp + o, tps)
+
+    barrier = pltpu.get_barrier_semaphore()
+    for dr in range(1, ring):
+        pl.semaphore_signal(barrier, 1, device_id=(sp_of(dr, 0), tp), device_id_type=MESH)
+    pl.semaphore_signal(barrier, 1, device_id=(partner, tp), device_id_type=MESH)
+    for o in range(1, tps):
+        pl.semaphore_signal(barrier, 1, device_id=(sp, tp_peer(o)), device_id_type=MESH)
+    pl.semaphore_wait(barrier, ring + tps - 1)
+
+    flat = [m for g in groups for m in g]
+    number = {m: i for i, m in enumerate(flat)}
+    arrival = {}
+    for (a, dr, rel, way) in flat:
+        to = {"R": (dr - 1, rel), "L": (dr + 1, rel), "Y": (dr, 1 - rel)}[way]
+        key = (a, to[0], to[1])
+        assert key not in arrival
+        arrival[key] = number[(a, dr, rel, way)]
+    waited = set()
+    copies = []
+
+    def exists(dr):
+        return (r + dr >= 0) & (r + dr < ring)
+
+    def slot(a, dr, rel):
+        s = sp_of(dr, rel)
+        if a == "D":
+            return down_all.at[s]
+        whole = gate_all if a == "G" else up_all
+        return whole.at[pl.ds(pl.multiple_of(s * kr, kr), kr), :]
+
+    inputs = {"G": gate_in, "U": up_in, "D": down_in}
+
+    def need(a, dr, rel):
+        key = (a, dr, rel)
+        if (dr == 0 and rel == 0) or key in waited:
+            return
+        waited.add(key)
+        m = arrival[key]
+
+        @pl.when(exists(dr))
+        def _():
+            here = slot(*key)
+            pltpu.make_async_remote_copy(
+                here, here, w_send.at[m], w_recv.at[m], device_id=(partner, tp), device_id_type=MESH
+            ).wait_recv()
+
+    def outgoing(message):
+        a, dr, rel, way = message
+        m = number[message]
+        return pltpu.make_async_remote_copy(
+            inputs[a] if dr == 0 and rel == 0 else slot(a, dr, rel),
+            slot(a, dr, rel),
+            w_send.at[m], w_recv.at[m],
+            device_id=(where[way], tp), device_id_type=MESH,
+        )
+
+    def goes(message):
+        ahead = {"R": r + 1 < ring, "L": r >= 1, "Y": r >= 0}[message[3]]
+        return exists(message[1]) & ahead
+
+    def pump(group):
+        for message in group:
+            need(*message[:3])
+
+            @pl.when(goes(message))
+            def _():
+                outgoing(message).start()
+
+            copies.append(message)
+
+    def need_all(a):
+        for dr in sorted(range(1 - ring, ring), key=abs):
+            for rel in (0, 1):
+                need(a, dr, rel)
+
+    first, down_y, early, middle, later, last_group = groups
+    pump(first)
+    locals_ = []
+    for i, a in enumerate("GUD"):
+        local = pltpu.make_async_copy(inputs[a], slot(a, 0, 0), own_sem.at[i])
+        local.start()
+        locals_.append(local)
+
+    states = local_scan(qp, kp, vp, strength, decay_pre, extra, rate, out_scr)
+    for h in range(heads):
+        x_send[h] = states[h].astype(BF16)
+    x_copy = pltpu.make_async_remote_copy(
+        x_send, x_part, x_sem.at[0], x_sem.at[1], device_id=(partner, tp), device_id_type=MESH)
+    x_copy.start()
+    pump(down_y)
+    x_copy.wait_recv()
+    combine(states, x_part, p, p_send)
+
+    def p_copy(k, to, at):
+        return pltpu.make_async_remote_copy(
+            p_send, p_recv.at[at], p_ssem.at[k], p_rsem.at[k],
+            device_id=(to, tp), device_id_type=MESH)
+
+    for k in range(1, ring):
+        @pl.when(r + k < ring)
+        def _():
+            p_copy(k, sp_of(k, 0), r).start()
+    pump(early)
+    for k in range(1, ring):
+        @pl.when(r - k >= 0)
+        def _():
+            p_copy(k, sp_of(-k, 0), r - k).wait_recv()
+    fold_states(r, p_recv, s_in, heads)
+    apply_state(p, x_part, s_in, out_scr, head_gain, gp, mixed, heads)
 
     def rows_of(t):
         return pl.ds(pl.multiple_of(t * own_rows, own_rows), own_rows)
@@ -388,7 +408,7 @@
             p_copy(k, sp_of(k, 0), r).wait_send()
 
 
-def body(n, tps, stream, qp, kp, vp, gp, strength, decay_pre, extra, rate, head_gain, w_out,
+def chain_body(n, tps, stream, qp, kp, vp, gp, strength, decay_pre, extra, rate, head_gain, w_out,
          feed_gain, gate_m, up_m, down_m):
     heads, tokens = strength.shape
     own, width = stream.shape
@@ -401,7 +421,7 @@
     hbm = pl.BlockSpec(memory_space=pl.ANY)
     peers = max(1, tps - 1)
     return pl.pallas_call(
-        functools.partial(kernel, n, tps, groups),
+        functools.partial(chain_kernel, n, tps, groups),
         out_shape=jax.ShapeDtypeStruct((own, width), BF16),
         in_specs=[vmem] * 12 + [hbm] * 3,
         out_specs=vmem,
@@ -432,6 +452,474 @@
       feed_gain[None, :], gate_m, up_m, down_m)
 
 
+def regions_of(ring, units):
+    tiles = units // 128
+    side = (tiles - 1) // 2 * 128
+    half, quarter = ring // 2, ring // 4
+    return {
+        "L": (0, half, 0, side),
+        "M": (quarter, half + quarter, side, units - side),
+        "H": (half, ring, units - side, units),
+    }
+
+
+def paired_kernel(
+    n, tps,
+    stream, qp, kp, vp, gp, strength, decay_pre, extra, rate, head_gain, feed_gain,
+    w_out, gate_in, up_in, down_in,
+    result,
+    gate_all, up_all, down_all, w_all, out_scr, x_send, x_part, p_send, p_recv, s_in, mixed, mix_all,
+    residual, rows_all, hidden, acc, acc2, acc3, fd_send, fd_recv, fx_send, fx_recv, fz_send, fz_recv,
+    w_send, w_recv, own_sem, x_sem, p_ssem, p_rsem, wo_ssem, wo_rsem, m_ssem, m_rsem, t_ssem, t_rsem,
+    fd_ssem, fd_rsem, fx_ssem, fx_rsem, fz_ssem, fz_rsem,
+):
+    ring = n // 2
+    half = ring // 2
+    sp = lax.axis_index("sp")
+    tp = lax.axis_index("tp")
+    r = sp // 2
+    p = lax.rem(sp, 2)
+    x = tp // 2
+    c = lax.rem(tp, 2)
+    zz = jnp.where(r >= half, 1, 0)
+    heads = strength.shape[0]
+    own_rows = stream.shape[0]
+    kr, units = gate_in.shape
+    width = stream.shape[1]
+    dc = down_in.shape[1]
+    MESH = pl.DeviceIdType.MESH
+    regions = regions_of(ring, units)
+    partner = r * 2 + 1 - p
+    mate = lax.rem(r + half, ring) * 2 + p
+    core = x * 2 + 1 - c
+    across = (1 - x) * 2 + c
+    diagonal = (1 - x) * 2 + 1 - c
+
+    def at(q):
+        return q * 2 + p
+
+    def remote(src, dst, ssem, rsem, sp_to, tp_to):
+        return pltpu.make_async_remote_copy(src, dst, ssem, rsem, device_id=(sp_to, tp_to), device_id_type=MESH)
+
+    inputs = {"G": gate_in, "U": up_in, "D": down_in}
+    keys = [(a, g, q, rel) for a in "GUD" for g in "LMH" for q in range(ring) for rel in (0, 1)]
+    number = {key: i for i, key in enumerate(keys)}
+
+    def slot(a, g, q, rel):
+        s = q * 2 + (p if rel == 0 else 1 - p)
+        c0, c1 = regions[g][2:]
+        if a == "D":
+            return down_all.at[s, c0:c1, :]
+        whole = gate_all if a == "G" else up_all
+        return whole.at[pl.ds(pl.multiple_of(s * kr, kr), kr), c0:c1]
+
+    def own(a, g):
+        c0, c1 = regions[g][2:]
+        return inputs[a].at[c0:c1, :] if a == "D" else inputs[a].at[:, c0:c1]
+
+    def member(g):
+        return (r >= regions[g][0]) & (r < regions[g][1])
+
+    own_copies = []
+    for i, a in enumerate("GUD"):
+        for j, g in enumerate("LMH"):
+            for q in range(*regions[g][:2]):
+                copy = pltpu.make_async_copy(own(a, g), slot(a, g, q, 0), own_sem.at[3 * i + j])
+                own_copies.append((r == q, copy))
+
+                @pl.when(r == q)
+                def _():
+                    copy.start()
+
+    w_local = pltpu.make_async_copy(w_out, w_all.at[tp], own_sem.at[9])
+    w_local.start()
+
+    barrier = pltpu.get_barrier_semaphore()
+    for k in range(1, ring):
+        pl.semaphore_signal(barrier, 1, device_id=(at(lax.rem(r + k, ring)), tp), device_id_type=MESH)
+    pl.semaphore_signal(barrier, 1, device_id=(partner, tp), device_id_type=MESH)
+    for k in range(1, tps):
+        pl.semaphore_signal(barrier, 1, device_id=(sp, lax.rem(tp + k, tps)), device_id_type=MESH)
+    pl.semaphore_wait(barrier, ring + tps - 1)
+
+    def detour(a, g, q, to):
+        lo, hi = regions[g][:2]
+        if g == "M" or hi - lo < 2:
+            return False
+        inner, outer = (hi - 1, hi - 2) if g == "L" else (lo, lo + 1)
+        return (q, to) == (outer, inner) or (a == "D" and (q, to) == (inner, outer))
+
+    sends = []
+    waited = set()
+
+    def send(cond, src, key, way, sp_to):
+        m = number[key]
+        dst = slot(key[0], key[1], key[2], key[3] if way != 3 else 0)
+
+        def make():
+            return remote(src, dst, w_send.at[m, way], w_recv.at[number[key[:3] + (1 if way == 3 else key[3],)]], sp_to, tp)
+
+        @pl.when(cond)
+        def _():
+            make().start()
+
+        sends.append((cond, make))
+
+    def y_cond(a, g, q, base):
+        cond = base
+        lo, hi = regions[g][:2]
+        for to in range(lo, hi):
+            if detour(a, g, q, to):
+                cond = cond & (r != to)
+        return cond
+
+    def own_sends(a, ways):
+        for g in "LMH":
+            lo, hi = regions[g][:2]
+            for q in range(ring):
+                key = (a, g, q, 0)
+                mine = r == q
+                if lo <= q < hi:
+                    here = slot(*key)
+                    if "l" in ways and q > lo:
+                        send(mine, here, key, 0, at(q - 1))
+                    if "r" in ways and q + 1 < hi:
+                        send(mine, here, key, 1, at(q + 1))
+                    if "y" in ways:
+                        send(mine, here, key, 3, partner)
+                elif "r" in ways and q < lo:
+                    send(mine, own(a, g), key, 2, at(lo))
+                elif "l" in ways and q >= hi:
+                    send(mine, own(a, g), key, 2, at(hi - 1))
+
+    def need(key):
+        if key in waited:
+            return
+        waited.add(key)
+        a, g, q, rel = key
+        cond = member(g)
+        if rel == 0:
+            cond = cond & (r != q)
+
+        @pl.when(cond)
+        def _():
+            here = slot(*key)
+            m = number[key]
+            remote(here, here, w_send.at[m, 0], w_recv.at[m], partner, tp).wait_recv()
+
+    def relay(a, g, q):
+        key = (a, g, q, 0)
+        lo, hi = regions[g][:2]
+        need(key)
+        here = slot(*key)
+        if min(q - 1, hi - 1) >= lo + 1:
+            send((r > lo) & (r < min(q, hi)), here, key, 0, at(r - 1))
+        if max(q + 1, lo) <= hi - 2:
+            send((r >= max(q + 1, lo)) & (r < hi - 1), here, key, 1, at(r + 1))
+        send(y_cond(a, g, q, member(g) & (r != q)), here, key, 3, partner)
+
+    def detours(a):
+        for g in "LH":
+            for q in range(*regions[g][:2]):
+                for to, way in ((q - 1, 0), (q + 1, 1)):
+                    if detour(a, g, q, to):
+                        key = (a, g, q, 1)
+                        m = number[key]
+                        here = slot(*key)
+                        cond = r == q
+
+                        @pl.when(cond)
+                        def _():
+                            remote(here, here, w_send.at[m, 0], w_recv.at[m], partner, tp).wait_recv()
+
+                        early.setdefault(key, []).append(q)
+                        send(cond, here, key, way, at(to))
+
+    early = {}
+    low = list(range(half - 1, -1, -1)) + list(range(half, ring))
+    high = [ring - 1 - q for q in low]
+    middle = sorted(range(ring), key=lambda q: abs(2 * q - ring + 1))
+
+    def relays(a, part):
+        cut = half if part == 0 else ring
+        start = 0 if part == 0 else half
+        for i in range(start, cut):
+            relay(a, "L", low[i])
+            relay(a, "H", high[i])
+            relay(a, "M", middle[i])
+
+    def finish(a, q, rel):
+        for g in "LMH":
+            key = (a, g, q, rel)
+            if key in waited:
+                continue
+            waited.add(key)
+            cond = member(g)
+            if rel == 0:
+                cond = cond & (r != q)
+            for done in early.get(key, []):
+                cond = cond & (r != done)
+
+            @pl.when(cond)
+            def _():
+                here = slot(*key)
+                m = number[key]
+                remote(here, here, w_send.at[m, 0], w_recv.at[m], partner, tp).wait_recv()
+
+    for cond, copy in own_copies:
+        @pl.when(cond)
+        def _():
+            copy.wait()
+    own_sends("G", "lry")
+    own_sends("U", "l")
+    w_local.wait()
+    w_x = remote(w_all.at[tp], w_all.at[tp], wo_ssem.at[0], wo_rsem.at[0], sp, across)
+    w_x.start()
+    w_d = remote(w_all.at[tp], w_all.at[tp], wo_ssem.at[1], wo_rsem.at[1], sp, core)
+    w_d.start()
+    w_xd = remote(w_all.at[across], w_all.at[across], wo_ssem.at[2], wo_rsem.at[2], sp, core)
+
+    states = local_scan(qp, kp, vp, strength, decay_pre, extra, rate, out_scr)
+    for h in range(heads):
+        x_send[h] = states[h].astype(BF16)
+    x_copy = remote(x_send, x_part, x_sem.at[0], x_sem.at[1], partner, tp)
+    x_copy.start()
+    own_sends("U", "y")
+    x_copy.wait_recv()
+    combine(states, x_part, p, p_send)
+
+    def p_copy(k, to, slot_at):
+        return remote(p_send, p_recv.at[slot_at], p_ssem.at[k], p_rsem.at[k], to, tp)
+
+    for k in range(1, ring):
+        @pl.when(r + k < ring)
+        def _():
+            p_copy(k, at(r + k), r).start()
+    own_sends("U", "r")
+    detours("G")
+    relays("G", 0)
+    w_x.wait_recv()
+    w_xd.start()
+    for k in range(1, ring):
+        @pl.when(r - k >= 0)
+        def _():
+            p_copy(k, at(r - k), r - k).wait_recv()
+    fold_states(r, p_recv, s_in, heads)
+    apply_state(p, x_part, s_in, out_scr, head_gain, gp, mixed, heads)
+
+    def token_rows(t):
+        return pl.ds(pl.multiple_of(t * own_rows, own_rows), own_rows)
+
+    mix_copies = []
+    for i, to in enumerate((across, diagonal, core)):
+        copy = remote(mixed.at[token_rows(to), :], mix_all.at[i], m_ssem.at[i], m_rsem.at[i], sp, to)
+        copy.start()
+        mix_copies.append((to, copy))
+    relays("G", 1)
+    total = dot1(mixed[token_rows(tp), :], w_all[tp]).astype(BF16).astype(F32)
+    w_d.wait_recv()
+    w_xd.wait_recv()
+    for i, (to, copy) in enumerate(mix_copies):
+        copy.wait_recv()
+        total = total + dot1(mix_all[i], w_all[to]).astype(BF16).astype(F32)
+    total = stream[...].astype(F32) + total
+    residual[...] = total
+    normed = (
+        total * lax.rsqrt(jnp.mean(total * total, axis=-1, keepdims=True) + EPSILON) * feed_gain[...]
+    ).astype(BF16)
+
+    def block_of(z_, x_, c_):
+        b = (c_ * 2 + x_) * 2 + z_
+        return rows_all.at[pl.ds(pl.multiple_of(b * own_rows, own_rows), own_rows), :]
+
+    b_own = (c * 2 + x) * 2 + zz
+    rows_all[pl.ds(pl.multiple_of(b_own * own_rows, own_rows), own_rows), :] = normed
+    t_copies = []
+
+    def token(i, block, sp_to, tp_to):
+        copy = remote(block, block, t_ssem.at[i], t_rsem.at[i], sp_to, tp_to)
+        copy.start()
+        t_copies.append(copy)
+
+    def token_wait(i, block):
+        remote(block, block, t_ssem.at[i], t_rsem.at[i], sp, across).wait_recv()
+
+    token(0, block_of(zz, x, c), mate, tp)
+    token(1, block_of(zz, x, c), sp, across)
+    token(2, block_of(zz, x, c), sp, core)
+    detours("U")
+    relays("U", 0)
+    token_wait(0, block_of(1 - zz, x, c))
+    token(3, block_of(1 - zz, x, c), sp, across)
+    token(4, block_of(1 - zz, x, c), sp, core)
+    token_wait(1, block_of(zz, 1 - x, c))
+    token(5, block_of(zz, 1 - x, c), sp, core)
+    own_sends("D", "lry")
+    relays("U", 1)
+    token_wait(3, block_of(1 - zz, 1 - x, c))
+    token(6, block_of(1 - zz, 1 - x, c), sp, core)
+    token_wait(2, block_of(zz, x, 1 - c))
+    token_wait(4, block_of(1 - zz, x, 1 - c))
+    token_wait(5, block_of(zz, 1 - x, 1 - c))
+    token_wait(6, block_of(1 - zz, 1 - x, 1 - c))
+    for a in "GU":
+        for rel in (0, 1):
+            for q in range(ring):
+                finish(a, q, rel)
+    detours("D")
+
+    has_m = member("M")
+    first = jnp.where(r < half, 0, jnp.where(has_m, regions["M"][2] // 128, regions["H"][2] // 128))
+    many = (regions["L"][3] - regions["L"][2]) // 128 + jnp.where(has_m, (regions["M"][3] - regions["M"][2]) // 128, 0)
+
+    def ffn_in(i, _):
+        lanes = pl.ds(pl.multiple_of((first + i) * 128, 128), 128)
+        both = dot1(rows_all[...], jnp.concatenate([gate_all[:, lanes], up_all[:, lanes]], axis=1))
+        hidden[:, pl.ds(pl.multiple_of(i * 128, 128), 128)] = (silu(both[:, :128]) * both[:, 128:]).astype(BF16)
+        return 0
+
+    lax.fori_loop(0, many, ffn_in, 0)
+    relays("D", 0)
+    relays("D", 1)
+
+    order = [(q, 0) for q in middle] + [(q, 1) for q in middle]
+    side = regions["L"][3]
+    mids = regions["M"][3] - regions["M"][2]
+    base = pl.multiple_of(first * 128, 128)
+    f_sends = []
+
+    def lanes_of(i):
+        q, rel = order[i]
+        s = q * 2 + (p if rel == 0 else 1 - p)
+        return s, pl.ds(pl.multiple_of(s * dc, dc), dc)
+
+    hop = 4 * own_rows
+
+    def stage_a(i):
+        q, rel = order[i]
+        finish("D", q, rel)
+        s, _ = lanes_of(i)
+
+        @pl.when(has_m)
+        def _():
+            acc[i] = dot1(hidden[...], down_all[s, pl.ds(base, side + mids), :])
+
+        @pl.when(jnp.logical_not(has_m))
+        def _():
+            acc[i] = dot1(hidden[:, :side], down_all[s, pl.ds(base, side), :])
+
+        fd_send[i] = acc[i, pl.ds(pl.multiple_of((1 - c) * hop, hop), hop), :].astype(BF16)
+        copy = remote(fd_send.at[i], fd_recv.at[i], fd_ssem.at[i], fd_rsem.at[i], sp, core)
+        copy.start()
+        f_sends.append(copy)
+
+    def stage_b(i):
+        f = remote(fd_send.at[i], fd_recv.at[i], fd_ssem.at[i], fd_rsem.at[i], sp, core)
+        f.wait_recv()
+        acc2[i] = acc[i, pl.ds(pl.multiple_of(c * hop, hop), hop), :] + fd_recv[i].astype(F32)
+        fx_send[i] = acc2[i, pl.ds(pl.multiple_of((1 - x) * (hop // 2), hop // 2), hop // 2), :].astype(BF16)
+        copy = remote(fx_send.at[i], fx_recv.at[i], fx_ssem.at[i], fx_rsem.at[i], sp, across)
+        copy.start()
+        f_sends.append(copy)
+
+    def stage_c(i):
+        f = remote(fx_send.at[i], fx_recv.at[i], fx_ssem.at[i], fx_rsem.at[i], sp, across)
+        f.wait_recv()
+        acc3[i] = acc2[i, pl.ds(pl.multiple_of(x * (hop // 2), hop // 2), hop // 2), :] + fx_recv[i].astype(F32)
+        fz_send[i] = acc3[i, pl.ds(pl.multiple_of((1 - zz) * own_rows, own_rows), own_rows), :].astype(BF16)
+        copy = remote(fz_send.at[i], fz_recv.at[i], fz_ssem.at[i], fz_rsem.at[i], mate, tp)
+        copy.start()
+        f_sends.append(copy)
+
+    def stage_d(i):
+        f = remote(fz_send.at[i], fz_recv.at[i], fz_ssem.at[i], fz_rsem.at[i], mate, tp)
+        f.wait_recv()
+        _, lanes = lanes_of(i)
+        ffn = acc3[i, pl.ds(pl.multiple_of(zz * own_rows, own_rows), own_rows), :] + fz_recv[i].astype(F32)
+        result[:, lanes] = (residual[:, lanes] + ffn).astype(BF16)
+
+    for i in range(n + 3):
+        if i < n:
+            stage_a(i)
+        if 0 <= i - 1 < n:
+            stage_b(i - 1)
+        if 0 <= i - 2 < n:
+            stage_c(i - 2)
+        if 0 <= i - 3 < n:
+            stage_d(i - 3)
+
+    for cond, make in sends:
+        @pl.when(cond)
+        def _():
+            make().wait_send()
+    for copy in [x_copy, w_x, w_d, w_xd] + [m for _, m in mix_copies] + t_copies + f_sends:
+        copy.wait_send()
+    for k in range(1, ring):
+        @pl.when(r + k < ring)
+        def _():
+            p_copy(k, at(r + k), r).wait_send()
+
+
+def paired_body(n, tps, stream, qp, kp, vp, gp, strength, decay_pre, extra, rate, head_gain, w_out,
+                feed_gain, gate_m, up_m, down_m):
+    heads, tokens = strength.shape
+    own, width = stream.shape
+    kr, units = gate_m.shape
+    dc = down_m.shape[1]
+    ring = n // 2
+    side = (units // 128 - 1) // 2 * 128
+    most = units - side
+    group = 2 * tps * own
+    dma = pltpu.SemaphoreType.DMA
+    vmem = pl.BlockSpec(memory_space=pltpu.VMEM)
+    hbm = pl.BlockSpec(memory_space=pl.ANY)
+    keys = 3 * 3 * ring * 2
+    return pl.pallas_call(
+        functools.partial(paired_kernel, n, tps),
+        out_shape=jax.ShapeDtypeStruct((own, width), BF16),
+        in_specs=[vmem] * 11 + [hbm] * 4,
+        out_specs=vmem,
+        scratch_shapes=[
+            pltpu.VMEM((kr * n, units), BF16),
+            pltpu.VMEM((kr * n, units), BF16),
+            pltpu.VMEM((n,) + down_m.shape, BF16),
+            pltpu.VMEM((tps,) + w_out.shape, BF16),
+            pltpu.VMEM((heads, tokens, 2 * HEAD), F32),
+            pltpu.VMEM((heads, HEAD, 2 * HEAD), BF16),
+            pltpu.VMEM((heads, HEAD, 2 * HEAD), BF16),
+            pltpu.VMEM((heads, HEAD, 2 * HEAD), BF16),
+            pltpu.VMEM((ring, heads, HEAD, 2 * HEAD), BF16),
+            pltpu.VMEM((heads, HEAD, HEAD), F32),
+            pltpu.VMEM((tokens, heads * HEAD), BF16),
+            pltpu.VMEM((tps - 1, own, heads * HEAD), BF16),
+            pltpu.VMEM((own, width), F32),
+            pltpu.VMEM((group, width), BF16),
+            pltpu.VMEM((group, most), BF16),
+            pltpu.VMEM((n, group, dc), F32),
+            pltpu.VMEM((n, group // 2, dc), F32),
+            pltpu.VMEM((n, group // 4, dc), F32),
+            pltpu.VMEM((n, group // 2, dc), BF16),
+            pltpu.VMEM((n, group // 2, dc), BF16),
+            pltpu.VMEM((n, group // 4, dc), BF16),
+            pltpu.VMEM((n, group // 4, dc), BF16),
+            pltpu.VMEM((n, group // 8, dc), BF16),
+            pltpu.VMEM((n, group // 8, dc), BF16),
+            dma((keys, 4)), dma((keys,)), dma((10,)), dma((2,)), dma((ring,)), dma((ring,)),
+            dma((3,)), dma((3,)), dma((3,)), dma((3,)), dma((7,)), dma((7,)),
+            dma((n,)), dma((n,)), dma((n,)), dma((n,)), dma((n,)), dma((n,)),
+        ],
+        compiler_params=pltpu.CompilerParams(
+            collective_id=0, has_side_effects=True, vmem_limit_bytes=60 * 1024 * 1024),
+    )(stream, qp, kp, vp, gp, strength, decay_pre, extra, rate[:, None], head_gain[None, :],
+      feed_gain[None, :], w_out, gate_m, up_m, down_m)
+
+
+def body(n, tps, *args):
+    ring = n // 2
+    short = ring % 4 == 0 and ring <= UNROLLED and tps == 4
+    return (paired_body if short else chain_body)(n, tps, *args)
+
+
 def solution(mesh):
     placed = (
         P(("sp", "tp"), None),

time: 214 us -> 157 us (0.73)
  Pallas kernels: 210 us -> 154 us
    pallas_call x1, Pallas kernels: 210 us -> 154 us  [paired_body(): pl.pallas_call(functools.partial(paired_kernel, n, tps), out_shape=jax.Sh...]
where the time goes in v1:
time: 157 us
  Pallas kernels  154 us (98%)
  local copies, waits for them, and re-layouts  3.07 us (2%)
    pallas_call x1, Pallas kernels, paired_body(): pl.pallas_call(functools.partial(paired_kernel, n, tps), out_shape=jax.Sh...  154 us

profile of v1, /device:TPU:0, one launch (start us, length us, event | category | flops | bytes accessed | tf_op | source)
XLA Modules:
  0.0 157.1 jit_solution(8821939721549087129)
XLA Ops:
  0.0 0.0 copy-start
  0.0 0.7 copy-done
  0.7 0.6 copy.16.rate
  1.3 154.0 %shard_map.145 = bf16[96,2048]{1,0:T(8,128)(2,1)} custom-call(bf16[96,2048]{1,0:T(8,128)(2,1)} %stream.1, bf16[384,256]{1,0:T(8,128)(2,1)} %qp.1, bf16[384,256]{1,0:T(8,128)(2,1)} %kp.1, bf16[384,256]{1,0:T(8,128)(2,1)} %vp.1, bf16[384,256]{1,0:T(8,128)(2,1)} %gp.1, bf16[2,384]{1,0:T(2,128)(2,1)} %strength.1, bf16[2,384]{1,0:T(2,128)(2,1)} %decay_pre.1, ...), custom_call_target="tpu_custom_call" | custom-call | tf_op jit(solution)/shard_map/pallas_call | solution.py:877
  155.3 1.8 %copy.18 = bf16[96,2048]{1,0:T(8,128)(2,1)} copy(bf16[96,2048]{1,0:T(8,128)(2,1)} %shard_map.145) | data formatting | bytes 786432
Async XLA Ops:
  0.0 0.7 copy-start

commit v2 on v1

--- a/solution.py
+++ b/solution.py
@@ -9,7 +9,7 @@
 
 HEAD = 128
 CHUNK = 128
-UNROLLED = 8
+UNROLLED = 4
 EPSILON = 1e-06
 F32 = jnp.float32
 BF16 = jnp.bfloat16
@@ -131,6 +131,23 @@
     lax.fori_loop(0, r, fold, 0)
 
 
+def fold_from_first(r, p_recv, s_in, heads):
+    s_in[...] = jnp.zeros_like(s_in)
+
+    @pl.when(r > 0)
+    def _():
+        for h in range(heads):
+            s_in[h] = p_recv[0, h, :, :HEAD].astype(F32)
+
+    def fold(i, _):
+        for h in range(heads):
+            got = p_recv[i, h].astype(F32)
+            s_in[h] = dot3(got[:, HEAD:], s_in[h]) + got[:, :HEAD]
+        return 0
+
+    lax.fori_loop(1, r, fold, 0)
+
+
 def apply_state(p, x_part, s_in, out_scr, head_gain, gp, mixed, heads):
     for h in range(heads):
         lanes = slice(h * HEAD, (h + 1) * HEAD)
@@ -502,8 +519,26 @@
         return pltpu.make_async_remote_copy(src, dst, ssem, rsem, device_id=(sp_to, tp_to), device_id_type=MESH)
 
     inputs = {"G": gate_in, "U": up_in, "D": down_in}
-    keys = [(a, g, q, rel) for a in "GUD" for g in "LMH" for q in range(ring) for rel in (0, 1)]
-    number = {key: i for i, key in enumerate(keys)}
+    def spans(g, k):
+        return (k >= regions[g][0]) & (k < regions[g][1])
+
+    taken = {"send": [], "recv": []}
+
+    def color(kind, users):
+        for i, held in enumerate(taken[kind]):
+            if not held & users:
+                held |= users
+                return i
+        taken[kind].append(set(users))
+        return len(taken[kind]) - 1
+
+    number = {}
+    for a in "GUD":
+        for g in "LMH":
+            for q in range(ring):
+                for rel in (0, 1):
+                    users = {k for k in range(ring) if spans(g, k) and (rel == 1 or k != q)}
+                    number[a, g, q, rel] = color("recv", users)
 
     def slot(a, g, q, rel):
         s = q * 2 + (p if rel == 0 else 1 - p)
@@ -518,7 +553,7 @@
         return inputs[a].at[c0:c1, :] if a == "D" else inputs[a].at[:, c0:c1]
 
     def member(g):
-        return (r >= regions[g][0]) & (r < regions[g][1])
+        return spans(g, r)
 
     own_copies = []
     for i, a in enumerate("GUD"):
@@ -547,131 +582,126 @@
         if g == "M" or hi - lo < 2:
             return False
         inner, outer = (hi - 1, hi - 2) if g == "L" else (lo, lo + 1)
-        return (q, to) == (outer, inner) or (a == "D" and (q, to) == (inner, outer))
+        return a != "G" and (q, to) == (outer, inner)
 
     sends = []
     waited = set()
 
     def send(cond, src, key, way, sp_to):
-        m = number[key]
-        dst = slot(key[0], key[1], key[2], key[3] if way != 3 else 0)
+        users = {k for k in range(ring) if cond(k)}
+        if not users:
+            return
+        m = color("send", users)
+        landing = key[:3] + (1,) if way == "y" else key
 
         def make():
-            return remote(src, dst, w_send.at[m, way], w_recv.at[number[key[:3] + (1 if way == 3 else key[3],)]], sp_to, tp)
-
-        @pl.when(cond)
+            return remote(src, slot(*key), w_send.at[m], w_recv.at[number[landing]], sp_to, tp)
+
+        @pl.when(cond(r))
         def _():
             make().start()
 
-        sends.append((cond, make))
-
-    def y_cond(a, g, q, base):
-        cond = base
-        lo, hi = regions[g][:2]
-        for to in range(lo, hi):
-            if detour(a, g, q, to):
-                cond = cond & (r != to)
-        return cond
-
-    def own_sends(a, ways):
+        sends.append((cond(r), make))
+
+    def forwards_y(a, g, q, k):
+        return spans(g, k) and not detour(a, g, q, k)
+
+    def own_sends(a, ways, only=None):
         for g in "LMH":
             lo, hi = regions[g][:2]
             for q in range(ring):
+                if only is not None and (q >= half) != only:
+                    continue
                 key = (a, g, q, 0)
-                mine = r == q
-                if lo <= q < hi:
-                    here = slot(*key)
-                    if "l" in ways and q > lo:
-                        send(mine, here, key, 0, at(q - 1))
-                    if "r" in ways and q + 1 < hi:
-                        send(mine, here, key, 1, at(q + 1))
-                    if "y" in ways:
-                        send(mine, here, key, 3, partner)
-                elif "r" in ways and q < lo:
-                    send(mine, own(a, g), key, 2, at(lo))
-                elif "l" in ways and q >= hi:
-                    send(mine, own(a, g), key, 2, at(hi - 1))
-
-    def need(key):
-        if key in waited:
-            return
-        waited.add(key)
-        a, g, q, rel = key
-        cond = member(g)
-        if rel == 0:
-            cond = cond & (r != q)
+                mine = functools.partial(lambda q, k: k == q, q)
+                inside = lo <= q < hi
+                here = slot(*key) if inside else own(a, g)
+                if inside and "y" in ways:
+                    send(mine, here, key, "y", partner)
+                if g == "M":
+                    targets = [to for to in range(lo, hi) if to != q]
+                elif inside:
+                    targets = [to for to in (q - 1, q + 1) if lo <= to < hi]
+                else:
+                    targets = [lo if q < lo else hi - 1]
+                for to in targets:
+                    way = "l" if to < q else "r"
+                    if (way if abs(q - to) == 1 else way.upper()) in ways:
+                        send(mine, here, key, way, at(to))
+
+    def arrived(key, cond):
+        here = slot(*key)
 
         @pl.when(cond)
         def _():
-            here = slot(*key)
-            m = number[key]
-            remote(here, here, w_send.at[m, 0], w_recv.at[m], partner, tp).wait_recv()
-
-    def relay(a, g, q):
+            remote(here, here, w_send.at[0], w_recv.at[number[key]], partner, tp).wait_recv()
+
+    def role_of(g, role, k):
+        lo, hi = regions[g][:2]
+        inner = hi - 1 if g == "L" else lo
+        return True if role is None else (k == inner) if role == "in" else (k != inner)
+
+    def relay(a, g, q, role):
         key = (a, g, q, 0)
         lo, hi = regions[g][:2]
-        need(key)
+        assert (key, role) not in waited
+        waited.add((key, role))
+
+        def holds(k):
+            return spans(g, k) & (k != q) & role_of(g, role, k)
+
+        if any(holds(k) for k in range(ring)):
+            arrived(key, holds(r))
         here = slot(*key)
-        if min(q - 1, hi - 1) >= lo + 1:
-            send((r > lo) & (r < min(q, hi)), here, key, 0, at(r - 1))
-        if max(q + 1, lo) <= hi - 2:
-            send((r >= max(q + 1, lo)) & (r < hi - 1), here, key, 1, at(r + 1))
-        send(y_cond(a, g, q, member(g) & (r != q)), here, key, 3, partner)
+        if g != "M":
+            send(lambda k: holds(k) & (k > lo) & (k < q), here, key, "l", at(r - 1))
+            send(lambda k: holds(k) & (k > q) & (k < hi - 1), here, key, "r", at(r + 1))
+        for k in range(lo, hi):
+            if holds(k) and forwards_y(a, g, q, k):
+                send(functools.partial(lambda k, kk: kk == k, k), here, key, "y", partner)
 
     def detours(a):
         for g in "LH":
             for q in range(*regions[g][:2]):
-                for to, way in ((q - 1, 0), (q + 1, 1)):
+                for to in (q - 1, q + 1):
                     if detour(a, g, q, to):
                         key = (a, g, q, 1)
-                        m = number[key]
-                        here = slot(*key)
-                        cond = r == q
-
-                        @pl.when(cond)
-                        def _():
-                            remote(here, here, w_send.at[m, 0], w_recv.at[m], partner, tp).wait_recv()
-
+                        arrived(key, r == q)
                         early.setdefault(key, []).append(q)
-                        send(cond, here, key, way, at(to))
+                        send(functools.partial(lambda q, k: k == q, q), slot(*key), key, "z", at(to))
 
     early = {}
     low = list(range(half - 1, -1, -1)) + list(range(half, ring))
-    high = [ring - 1 - q for q in low]
-    middle = sorted(range(ring), key=lambda q: abs(2 * q - ring + 1))
-
-    def relays(a, part):
-        cut = half if part == 0 else ring
-        start = 0 if part == 0 else half
-        for i in range(start, cut):
-            relay(a, "L", low[i])
-            relay(a, "H", high[i])
-            relay(a, "M", middle[i])
+
+    def relays(a, role, g, *steps):
+        for i in steps:
+            relay(a, g, low[i] if g == "L" else ring - 1 - low[i], role)
+
+    def middles(a):
+        for q in range(ring):
+            relay(a, "M", q, None)
 
     def finish(a, q, rel):
         for g in "LMH":
             key = (a, g, q, rel)
-            if key in waited:
+            if rel == 1:
+                cond = member(g)
+                for done in early.get(key, []):
+                    cond = cond & (r != done)
+                arrived(key, cond)
                 continue
-            waited.add(key)
-            cond = member(g)
-            if rel == 0:
-                cond = cond & (r != q)
-            for done in early.get(key, []):
-                cond = cond & (r != done)
-
-            @pl.when(cond)
-            def _():
-                here = slot(*key)
-                m = number[key]
-                remote(here, here, w_send.at[m, 0], w_recv.at[m], partner, tp).wait_recv()
+            for role in (None,) if g == "M" else ("in", "out"):
+                if (key, role) not in waited:
+                    waited.add((key, role))
+                    mine = member(g) & (r != q)
+                    arrived(key, mine & role_of(g, role, r))
 
     for cond, copy in own_copies:
         @pl.when(cond)
         def _():
             copy.wait()
+    own_sends("G", "LR")
     own_sends("G", "lry")
-    own_sends("U", "l")
     w_local.wait()
     w_x = remote(w_all.at[tp], w_all.at[tp], wo_ssem.at[0], wo_rsem.at[0], sp, across)
     w_x.start()
@@ -684,27 +714,43 @@
         x_send[h] = states[h].astype(BF16)
     x_copy = remote(x_send, x_part, x_sem.at[0], x_sem.at[1], partner, tp)
     x_copy.start()
+    own_sends("U", "lL")
+    own_sends("U", "r", True)
+    x_copy.wait_recv()
     own_sends("U", "y")
-    x_copy.wait_recv()
     combine(states, x_part, p, p_send)
 
     def p_copy(k, to, slot_at):
         return remote(p_send, p_recv.at[slot_at], p_ssem.at[k], p_rsem.at[k], to, tp)
 
-    for k in range(1, ring):
-        @pl.when(r + k < ring)
+    def p_first(k, to):
+        return remote(p_send.at[:, :, :HEAD], p_recv.at[0, :, :, :HEAD], p_ssem.at[k], p_rsem.at[k], to, tp)
+
+    for k in range(ring - 1, 0, -1):
+        @pl.when(r == 0)
+        def _():
+            p_first(k, at(k)).start()
+
+        @pl.when((r > 0) & (r + k < ring))
         def _():
             p_copy(k, at(r + k), r).start()
-    own_sends("U", "r")
-    detours("G")
-    relays("G", 0)
+    relays("G", "out", "L", 0)
+    relays("G", "out", "H", 0)
+    relays("G", "in", "L", 1, 2, 3)
+    relays("G", "in", "H", 1)
+    own_sends("D", "y")
     w_x.wait_recv()
     w_xd.start()
     for k in range(1, ring):
-        @pl.when(r - k >= 0)
+        @pl.when(r == k)
+        def _():
+            p_first(k, at(0)).wait_recv()
+
+        @pl.when(r - k > 0)
         def _():
             p_copy(k, at(r - k), r - k).wait_recv()
-    fold_states(r, p_recv, s_in, heads)
+    relays("G", "in", "H", 2)
+    fold_from_first(r, p_recv, s_in, heads)
     apply_state(p, x_part, s_in, out_scr, head_gain, gp, mixed, heads)
 
     def token_rows(t):
@@ -715,7 +761,19 @@
         copy = remote(mixed.at[token_rows(to), :], mix_all.at[i], m_ssem.at[i], m_rsem.at[i], sp, to)
         copy.start()
         mix_copies.append((to, copy))
-    relays("G", 1)
+    for k in range(1, ring):
+        @pl.when(r == 0)
+        def _():
+            p_first(k, at(k)).wait_send()
+
+        @pl.when((r > 0) & (r + k < ring))
+        def _():
+            p_copy(k, at(r + k), r).wait_send()
+    own_sends("U", "R")
+    own_sends("U", "r", False)
+    relays("G", "out", "L", 2)
+    relays("G", "out", "H", 2)
+    relays("U", "out", "L", 0)
     total = dot1(mixed[token_rows(tp), :], w_all[tp]).astype(BF16).astype(F32)
     w_d.wait_recv()
     w_xd.wait_recv()
@@ -747,17 +805,36 @@
     token(0, block_of(zz, x, c), mate, tp)
     token(1, block_of(zz, x, c), sp, across)
     token(2, block_of(zz, x, c), sp, core)
+    relays("G", "out", "L", 3)
+    relays("G", "in", "H", 3)
+    relays("U", "in", "L", 1, 2)
+    relays("U", "in", "H", 1)
+    relays("U", "out", "H", 0)
+    middles("G")
     detours("U")
-    relays("U", 0)
+    token_wait(1, block_of(zz, 1 - x, c))
+    token(5, block_of(zz, 1 - x, c), sp, core)
+    own_sends("D", "LR")
+    own_sends("D", "lr")
+    relays("G", "out", "H", 3)
+    relays("U", "in", "H", 2)
+    relays("U", "in", "L", 3)
+    relays("U", "out", "L", 2)
     token_wait(0, block_of(1 - zz, x, c))
     token(3, block_of(1 - zz, x, c), sp, across)
     token(4, block_of(1 - zz, x, c), sp, core)
-    token_wait(1, block_of(zz, 1 - x, c))
-    token(5, block_of(zz, 1 - x, c), sp, core)
-    own_sends("D", "lry")
-    relays("U", 1)
+    relays("U", "in", "H", 3)
+    relays("U", "out", "L", 3)
+    relays("U", "out", "H", 2)
+    middles("U")
     token_wait(3, block_of(1 - zz, 1 - x, c))
     token(6, block_of(1 - zz, 1 - x, c), sp, core)
+    relays("U", "out", "H", 3)
+    relays("D", "out", "L", 0)
+    relays("D", "out", "H", 0)
+    relays("D", "in", "L", 1, 2)
+    relays("D", "in", "H", 1)
+    detours("D")
     token_wait(2, block_of(zz, x, 1 - c))
     token_wait(4, block_of(1 - zz, x, 1 - c))
     token_wait(5, block_of(zz, 1 - x, 1 - c))
@@ -766,7 +843,6 @@
         for rel in (0, 1):
             for q in range(ring):
                 finish(a, q, rel)
-    detours("D")
 
     has_m = member("M")
     first = jnp.where(r < half, 0, jnp.where(has_m, regions["M"][2] // 128, regions["H"][2] // 128))
@@ -779,9 +855,7 @@
         return 0
 
     lax.fori_loop(0, many, ffn_in, 0)
-    relays("D", 0)
-    relays("D", 1)
-
+    middle = sorted(range(ring), key=lambda q: abs(2 * q - ring + 1))
     order = [(q, 0) for q in middle] + [(q, 1) for q in middle]
     side = regions["L"][3]
     mids = regions["M"][3] - regions["M"][2]
@@ -838,15 +912,23 @@
         ffn = acc3[i, pl.ds(pl.multiple_of(zz * own_rows, own_rows), own_rows), :] + fz_recv[i].astype(F32)
         result[:, lanes] = (residual[:, lanes] + ffn).astype(BF16)
 
-    for i in range(n + 3):
+    ahead = {
+        0: (("in", "H", 2), ("in", "L", 3), ("out", "L", 2), ("out", "H", 2)),
+        2: (("in", "H", 3), ("out", "L", 3), ("out", "H", 3)),
+    }
+    for i in range(n + 5):
+        for role, g, step in ahead.get(i, ()):
+            relays("D", role, g, step)
+        if i == 0:
+            middles("D")
         if i < n:
             stage_a(i)
         if 0 <= i - 1 < n:
             stage_b(i - 1)
-        if 0 <= i - 2 < n:
-            stage_c(i - 2)
         if 0 <= i - 3 < n:
-            stage_d(i - 3)
+            stage_c(i - 3)
+        if 0 <= i - 5 < n:
+            stage_d(i - 5)
 
     for cond, make in sends:
         @pl.when(cond)
@@ -854,10 +936,7 @@
             make().wait_send()
     for copy in [x_copy, w_x, w_d, w_xd] + [m for _, m in mix_copies] + t_copies + f_sends:
         copy.wait_send()
-    for k in range(1, ring):
-        @pl.when(r + k < ring)
-        def _():
-            p_copy(k, at(r + k), r).wait_send()
+    assert max(len(taken["send"]), len(taken["recv"])) <= w_send.shape[0]
 
 
 def paired_body(n, tps, stream, qp, kp, vp, gp, strength, decay_pre, extra, rate, head_gain, w_out,
@@ -873,7 +952,7 @@
     dma = pltpu.SemaphoreType.DMA
     vmem = pl.BlockSpec(memory_space=pltpu.VMEM)
     hbm = pl.BlockSpec(memory_space=pl.ANY)
-    keys = 3 * 3 * ring * 2
+    count = 12 * ring
     return pl.pallas_call(
         functools.partial(paired_kernel, n, tps),
         out_shape=jax.ShapeDtypeStruct((own, width), BF16),
@@ -904,7 +983,7 @@
             pltpu.VMEM((n, group // 4, dc), BF16),
             pltpu.VMEM((n, group // 8, dc), BF16),
             pltpu.VMEM((n, group // 8, dc), BF16),
-            dma((keys, 4)), dma((keys,)), dma((10,)), dma((2,)), dma((ring,)), dma((ring,)),
+            dma((count,)), dma((count,)), dma((10,)), dma((2,)), dma((ring,)), dma((ring,)),
             dma((3,)), dma((3,)), dma((3,)), dma((3,)), dma((7,)), dma((7,)),
             dma((n,)), dma((n,)), dma((n,)), dma((n,)), dma((n,)), dma((n,)),
         ],

time: 157 us -> 134 us (0.85)
  the two profiles are of different devices: /device:TPU:0 before, /device:TPU:8 now
where the time goes in v2:
time: 134 us; the launch traced here: 133 us
  Pallas kernels  130 us (97%)
  local copies, waits for them, and re-layouts  3.07 us (2%)
    pallas_call x1, Pallas kernels, paired_body(): pl.pallas_call(functools.partial(paired_kernel, n, tps), out_shape=jax.Sh...  130 us

profile of v2, /device:TPU:8, one launch (start us, length us, event | category | flops | bytes accessed | tf_op | source)
XLA Modules:
  0.0 133.4 jit_solution(7507608798281832815)
XLA Ops:
  0.0 0.0 copy-start
  0.0 0.7 copy-done
  0.7 0.6 copy.16.rate
  1.3 130.3 %shard_map.145 = bf16[96,2048]{1,0:T(8,128)(2,1)} custom-call(bf16[96,2048]{1,0:T(8,128)(2,1)} %stream.1, bf16[384,256]{1,0:T(8,128)(2,1)} %qp.1, bf16[384,256]{1,0:T(8,128)(2,1)} %kp.1, bf16[384,256]{1,0:T(8,128)(2,1)} %vp.1, bf16[384,256]{1,0:T(8,128)(2,1)} %gp.1, bf16[2,384]{1,0:T(2,128)(2,1)} %strength.1, bf16[2,384]{1,0:T(2,128)(2,1)} %decay_pre.1, ...), custom_call_target="tpu_custom_call" | custom-call | tf_op jit(solution)/shard_map/pallas_call | solution.py:956
  131.6 1.8 %copy.18 = bf16[96,2048]{1,0:T(8,128)(2,1)} copy(bf16[96,2048]{1,0:T(8,128)(2,1)} %shard_map.145) | data formatting | bytes 786432
Async XLA Ops:
  0.0 0.7 copy-start

commit v3 on v2

--- a/solution.py
+++ b/solution.py
@@ -50,7 +50,7 @@
     beta = jax.nn.sigmoid(strength[...].astype(F32))
     pre = decay_pre[...].astype(F32)
     soft = jnp.maximum(pre, 0.0) + jnp.log1p(jnp.exp(-jnp.abs(pre)))
-    log_decay = -rate[...] * soft + extra[...]
+    log_decay = -rate * soft + extra[...]
 
     pairs = [(h, c) for c in range(chunks) for h in range(heads)]
     data = {}
@@ -131,23 +131,6 @@
     lax.fori_loop(0, r, fold, 0)
 
 
-def fold_from_first(r, p_recv, s_in, heads):
-    s_in[...] = jnp.zeros_like(s_in)
-
-    @pl.when(r > 0)
-    def _():
-        for h in range(heads):
-            s_in[h] = p_recv[0, h, :, :HEAD].astype(F32)
-
-    def fold(i, _):
-        for h in range(heads):
-            got = p_recv[i, h].astype(F32)
-            s_in[h] = dot3(got[:, HEAD:], s_in[h]) + got[:, :HEAD]
-        return 0
-
-    lax.fori_loop(1, r, fold, 0)
-
-
 def apply_state(p, x_part, s_in, out_scr, head_gain, gp, mixed, heads):
     for h in range(heads):
         lanes = slice(h * HEAD, (h + 1) * HEAD)
@@ -305,7 +288,7 @@
         local.start()
         locals_.append(local)
 
-    states = local_scan(qp, kp, vp, strength, decay_pre, extra, rate, out_scr)
+    states = local_scan(qp, kp, vp, strength, decay_pre, extra, rate[...], out_scr)
     for h in range(heads):
         x_send[h] = states[h].astype(BF16)
     x_copy = pltpu.make_async_remote_copy(
@@ -482,14 +465,23 @@
 
 def paired_kernel(
     n, tps,
-    stream, qp, kp, vp, gp, strength, decay_pre, extra, rate, head_gain, feed_gain,
+    stream_in, qp_in, kp_in, vp_in, gp_in, strength_in, decay_in, extra_in, rate_in, head_gain_in, feed_gain_in,
     w_out, gate_in, up_in, down_in,
     result,
-    gate_all, up_all, down_all, w_all, out_scr, x_send, x_part, p_send, p_recv, s_in, mixed, mix_all,
+    stream, qp, kp, vp, gp, strength, decay_pre, extra, rate, head_gain, feed_gain, in_sem,
+    gate_all, up_all, down_all, w_all, out_scr, x_send, x_part, p_send, s_send, s_got, s_in, mixed, mix_all,
     residual, rows_all, hidden, acc, acc2, acc3, fd_send, fd_recv, fx_send, fx_recv, fz_send, fz_recv,
-    w_send, w_recv, own_sem, x_sem, p_ssem, p_rsem, wo_ssem, wo_rsem, m_ssem, m_rsem, t_ssem, t_rsem,
+    w_send, w_recv, own_sem, x_sem, s_sem, wo_ssem, wo_rsem, m_ssem, m_rsem, t_ssem, t_rsem,
     fd_ssem, fd_rsem, fx_ssem, fx_rsem, fz_ssem, fz_rsem,
 ):
+    loads = []
+    for i, (src, dst) in enumerate((
+        (strength_in, strength), (decay_in, decay_pre), (extra_in, extra), (rate_in, rate), (kp_in, kp), (qp_in, qp),
+        (vp_in, vp), (gp_in, gp), (stream_in, stream), (head_gain_in, head_gain), (feed_gain_in, feed_gain),
+    )):
+        load = pltpu.make_async_copy(src, dst, in_sem.at[i])
+        load.start()
+        loads.append(load)
     ring = n // 2
     half = ring // 2
     sp = lax.axis_index("sp")
@@ -610,7 +602,7 @@
         for g in "LMH":
             lo, hi = regions[g][:2]
             for q in range(ring):
-                if only is not None and (q >= half) != only:
+                if only is not None and q not in only:
                     continue
                 key = (a, g, q, 0)
                 mine = functools.partial(lambda q, k: k == q, q)
@@ -701,56 +693,68 @@
         def _():
             copy.wait()
     own_sends("G", "LR")
-    own_sends("G", "lry")
+    own_sends("G", "ly")
+    own_sends("G", "r", range(1, ring))
     w_local.wait()
     w_x = remote(w_all.at[tp], w_all.at[tp], wo_ssem.at[0], wo_rsem.at[0], sp, across)
-    w_x.start()
+    w_half = w_out.shape[0] // 2
+    w_part = w_all.at[tp, :w_half, :]
+    remote(w_part, w_part, wo_ssem.at[0], wo_rsem.at[0], sp, across).start()
     w_d = remote(w_all.at[tp], w_all.at[tp], wo_ssem.at[1], wo_rsem.at[1], sp, core)
     w_d.start()
     w_xd = remote(w_all.at[across], w_all.at[across], wo_ssem.at[2], wo_rsem.at[2], sp, core)
 
-    states = local_scan(qp, kp, vp, strength, decay_pre, extra, rate, out_scr)
+    for load in loads:
+        load.wait()
+    square = (heads, heads)
+    same = lax.broadcasted_iota(jnp.int32, square, 0) == lax.broadcasted_iota(jnp.int32, square, 1)
+    rates = jnp.sum(jnp.where(same, jnp.broadcast_to(rate[...], square), 0.0), axis=1, keepdims=True)
+    states = local_scan(qp, kp, vp, strength, decay_pre, extra, rates, out_scr)
     for h in range(heads):
         x_send[h] = states[h].astype(BF16)
     x_copy = remote(x_send, x_part, x_sem.at[0], x_sem.at[1], partner, tp)
     x_copy.start()
     own_sends("U", "lL")
-    own_sends("U", "r", True)
+    own_sends("U", "r", range(half, ring))
     x_copy.wait_recv()
+    combine(states, x_part, p, p_send)
+
+    def s_copy(src, to):
+        return remote(src, s_got, s_sem.at[0], s_sem.at[1], at(to), tp)
+
+    s_in[...] = jnp.zeros_like(s_in)
+
+    @pl.when(r == 0)
+    def _():
+        s_copy(p_send.at[:, :, :HEAD], 1).start()
+
+    own_sends("G", "r", range(1))
+    w_rest = w_all.at[tp, w_half:, :]
+    remote(w_rest, w_rest, wo_ssem.at[0], wo_rsem.at[0], sp, across).start()
     own_sends("U", "y")
-    combine(states, x_part, p, p_send)
-
-    def p_copy(k, to, slot_at):
-        return remote(p_send, p_recv.at[slot_at], p_ssem.at[k], p_rsem.at[k], to, tp)
-
-    def p_first(k, to):
-        return remote(p_send.at[:, :, :HEAD], p_recv.at[0, :, :, :HEAD], p_ssem.at[k], p_rsem.at[k], to, tp)
-
-    for k in range(ring - 1, 0, -1):
-        @pl.when(r == 0)
-        def _():
-            p_first(k, at(k)).start()
-
-        @pl.when((r > 0) & (r + k < ring))
-        def _():
-            p_copy(k, at(r + k), r).start()
     relays("G", "out", "L", 0)
     relays("G", "out", "H", 0)
-    relays("G", "in", "L", 1, 2, 3)
     relays("G", "in", "H", 1)
+
+    @pl.when(r > 0)
+    def _():
+        s_copy(s_send, 0).wait_recv()
+        for h in range(heads):
+            s_in[h] = s_got[h].astype(F32)
+
+    @pl.when((r > 0) & (r + 1 < ring))
+    def _():
+        for h in range(heads):
+            both = p_send[h].astype(F32)
+            s_send[h] = (dot3(both[:, HEAD:], s_in[h]) + both[:, :HEAD]).astype(BF16)
+        s_copy(s_send, lax.rem(r + 1, ring)).start()
+
+    own_sends("U", "r", range(1, half))
+    relays("G", "in", "L", 2, 3)
     own_sends("D", "y")
     w_x.wait_recv()
     w_xd.start()
-    for k in range(1, ring):
-        @pl.when(r == k)
-        def _():
-            p_first(k, at(0)).wait_recv()
-
-        @pl.when(r - k > 0)
-        def _():
-            p_copy(k, at(r - k), r - k).wait_recv()
-    relays("G", "in", "H", 2)
-    fold_from_first(r, p_recv, s_in, heads)
+    own_sends("U", "R")
     apply_state(p, x_part, s_in, out_scr, head_gain, gp, mixed, heads)
 
     def token_rows(t):
@@ -761,18 +765,9 @@
         copy = remote(mixed.at[token_rows(to), :], mix_all.at[i], m_ssem.at[i], m_rsem.at[i], sp, to)
         copy.start()
         mix_copies.append((to, copy))
-    for k in range(1, ring):
-        @pl.when(r == 0)
-        def _():
-            p_first(k, at(k)).wait_send()
-
-        @pl.when((r > 0) & (r + k < ring))
-        def _():
-            p_copy(k, at(r + k), r).wait_send()
-    own_sends("U", "R")
-    own_sends("U", "r", False)
+    relays("G", "in", "H", 2, 3)
+    relays("G", "in", "L", 1)
     relays("G", "out", "L", 2)
-    relays("G", "out", "H", 2)
     relays("U", "out", "L", 0)
     total = dot1(mixed[token_rows(tp), :], w_all[tp]).astype(BF16).astype(F32)
     w_d.wait_recv()
@@ -805,36 +800,40 @@
     token(0, block_of(zz, x, c), mate, tp)
     token(1, block_of(zz, x, c), sp, across)
     token(2, block_of(zz, x, c), sp, core)
+    own_sends("U", "r", range(1))
     relays("G", "out", "L", 3)
-    relays("G", "in", "H", 3)
-    relays("U", "in", "L", 1, 2)
+    relays("G", "out", "H", 2)
+    relays("U", "in", "L", 2)
     relays("U", "in", "H", 1)
     relays("U", "out", "H", 0)
     middles("G")
     detours("U")
+    relays("U", "in", "L", 3)
     token_wait(1, block_of(zz, 1 - x, c))
     token(5, block_of(zz, 1 - x, c), sp, core)
+    relays("G", "out", "H", 3)
+    relays("U", "in", "H", 2, 3)
+    own_sends("D", "lr")
+    relays("U", "out", "L", 2)
+    relays("U", "out", "H", 2)
     own_sends("D", "LR")
-    own_sends("D", "lr")
-    relays("G", "out", "H", 3)
-    relays("U", "in", "H", 2)
-    relays("U", "in", "L", 3)
-    relays("U", "out", "L", 2)
+    relays("U", "in", "L", 1)
+    relays("U", "out", "L", 3)
+    relays("U", "out", "H", 3)
     token_wait(0, block_of(1 - zz, x, c))
     token(3, block_of(1 - zz, x, c), sp, across)
     token(4, block_of(1 - zz, x, c), sp, core)
-    relays("U", "in", "H", 3)
-    relays("U", "out", "L", 3)
-    relays("U", "out", "H", 2)
     middles("U")
     token_wait(3, block_of(1 - zz, 1 - x, c))
     token(6, block_of(1 - zz, 1 - x, c), sp, core)
-    relays("U", "out", "H", 3)
     relays("D", "out", "L", 0)
     relays("D", "out", "H", 0)
     relays("D", "in", "L", 1, 2)
     relays("D", "in", "H", 1)
     detours("D")
+    relays("D", "in", "H", 2)
+    relays("D", "in", "L", 3)
+    relays("D", "in", "H", 3)
     token_wait(2, block_of(zz, x, 1 - c))
     token_wait(4, block_of(1 - zz, x, 1 - c))
     token_wait(5, block_of(zz, 1 - x, 1 - c))
@@ -913,8 +912,8 @@
         result[:, lanes] = (residual[:, lanes] + ffn).astype(BF16)
 
     ahead = {
-        0: (("in", "H", 2), ("in", "L", 3), ("out", "L", 2), ("out", "H", 2)),
-        2: (("in", "H", 3), ("out", "L", 3), ("out", "H", 3)),
+        0: (("out", "L", 2), ("out", "H", 2)),
+        2: (("out", "L", 3), ("out", "H", 3)),
     }
     for i in range(n + 5):
         for role, g, step in ahead.get(i, ()):
@@ -936,6 +935,15 @@
             make().wait_send()
     for copy in [x_copy, w_x, w_d, w_xd] + [m for _, m in mix_copies] + t_copies + f_sends:
         copy.wait_send()
+
+    @pl.when(r == 0)
+    def _():
+        s_copy(p_send.at[:, :, :HEAD], 1).wait_send()
+
+    @pl.when((r > 0) & (r + 1 < ring))
+    def _():
+        s_copy(s_send, 0).wait_send()
+
     assert max(len(taken["send"]), len(taken["recv"])) <= w_send.shape[0]
 
 
@@ -953,12 +961,14 @@
     vmem = pl.BlockSpec(memory_space=pltpu.VMEM)
     hbm = pl.BlockSpec(memory_space=pl.ANY)
     count = 12 * ring
+    arrays = (stream, qp, kp, vp, gp, strength, decay_pre, extra, rate[None, :], head_gain[None, :], feed_gain[None, :])
     return pl.pallas_call(
         functools.partial(paired_kernel, n, tps),
         out_shape=jax.ShapeDtypeStruct((own, width), BF16),
-        in_specs=[vmem] * 11 + [hbm] * 4,
+        in_specs=[hbm] * 15,
         out_specs=vmem,
         scratch_shapes=[
+            *(pltpu.VMEM(a.shape, a.dtype) for a in arrays), dma((len(arrays),)),
             pltpu.VMEM((kr * n, units), BF16),
             pltpu.VMEM((kr * n, units), BF16),
             pltpu.VMEM((n,) + down_m.shape, BF16),
@@ -967,7 +977,8 @@
             pltpu.VMEM((heads, HEAD, 2 * HEAD), BF16),
             pltpu.VMEM((heads, HEAD, 2 * HEAD), BF16),
             pltpu.VMEM((heads, HEAD, 2 * HEAD), BF16),
-            pltpu.VMEM((ring, heads, HEAD, 2 * HEAD), BF16),
+            pltpu.VMEM((heads, HEAD, HEAD), BF16),
+            pltpu.VMEM((heads, HEAD, HEAD), BF16),
             pltpu.VMEM((heads, HEAD, HEAD), F32),
             pltpu.VMEM((tokens, heads * HEAD), BF16),
             pltpu.VMEM((tps - 1, own, heads * HEAD), BF16),
@@ -983,14 +994,13 @@
             pltpu.VMEM((n, group // 4, dc), BF16),
             pltpu.VMEM((n, group // 8, dc), BF16),
             pltpu.VMEM((n, group // 8, dc), BF16),
-            dma((count,)), dma((count,)), dma((10,)), dma((2,)), dma((ring,)), dma((ring,)),
+            dma((count,)), dma((count,)), dma((10,)), dma((2,)), dma((2,)),
             dma((3,)), dma((3,)), dma((3,)), dma((3,)), dma((7,)), dma((7,)),
             dma((n,)), dma((n,)), dma((n,)), dma((n,)), dma((n,)), dma((n,)),
         ],
         compiler_params=pltpu.CompilerParams(
             collective_id=0, has_side_effects=True, vmem_limit_bytes=60 * 1024 * 1024),
-    )(stream, qp, kp, vp, gp, strength, decay_pre, extra, rate[:, None], head_gain[None, :],
-      feed_gain[None, :], w_out, gate_m, up_m, down_m)
+    )(*arrays, w_out, gate_m, up_m, down_m)
 
 
 def body(n, tps, *args):

time: 134 us -> 119 us (0.89)
  the two profiles are of different devices: /device:TPU:8 before, /device:TPU:0 now
where the time goes in v3:
time: 119 us
  Pallas kernels  117 us (98%)
  local copies, waits for them, and re-layouts  1.77 us (1%)
    pallas_call x1, Pallas kernels, paired_body(): pl.pallas_call(functools.partial(paired_kernel, n, tps), out_shape=jax.Sh...  117 us

profile of v3, /device:TPU:0, one launch (start us, length us, event | category | flops | bytes accessed | tf_op | source)
XLA Modules:
  0.0 119.0 jit_solution(2218758835024513917)
XLA Ops:
  0.0 117.2 %shard_map.145 = bf16[96,2048]{1,0:T(8,128)(2,1)} custom-call(bf16[96,2048]{1,0:T(8,128)(2,1)} %stream_in.1, bf16[384,256]{1,0:T(8,128)(2,1)} %qp_in.1, bf16[384,256]{1,0:T(8,128)(2,1)} %kp_in.1, bf16[384,256]{1,0:T(8,128)(2,1)} %vp_in.1, bf16[384,256]{1,0:T(8,128)(2,1)} %gp_in.1, bf16[2,384]{1,0:T(2,128)(2,1)} %strength_in.1, bf16[2,384]{1,0:T(2,128)(2,1)} %decay_in.1, ...), custom_call_target="tpu_custom_call" | custom-call | tf_op jit(solution)/shard_map/pallas_call | solution.py:965
  117.2 1.8 %copy.17 = bf16[96,2048]{1,0:T(8,128)(2,1)} copy(bf16[96,2048]{1,0:T(8,128)(2,1)} %shard_map.145) | data formatting | bytes 786432

commit v4 on v3

--- a/solution.py
+++ b/solution.py
@@ -751,7 +751,7 @@
 
     own_sends("U", "r", range(1, half))
     relays("G", "in", "L", 2, 3)
-    own_sends("D", "y")
+    own_sends("D", "y", [q for q in range(ring) if q not in (half - 1, half)])
     w_x.wait_recv()
     w_xd.start()
     own_sends("U", "R")
@@ -804,7 +804,6 @@
     relays("G", "out", "L", 3)
     relays("G", "out", "H", 2)
     relays("U", "in", "L", 2)
-    relays("U", "in", "H", 1)
     relays("U", "out", "H", 0)
     middles("G")
     detours("U")
@@ -817,23 +816,21 @@
     relays("U", "out", "L", 2)
     relays("U", "out", "H", 2)
     own_sends("D", "LR")
-    relays("U", "in", "L", 1)
-    relays("U", "out", "L", 3)
-    relays("U", "out", "H", 3)
     token_wait(0, block_of(1 - zz, x, c))
     token(3, block_of(1 - zz, x, c), sp, across)
     token(4, block_of(1 - zz, x, c), sp, core)
+    relays("U", "out", "L", 3)
+    relays("U", "out", "H", 3)
     middles("U")
+    own_sends("D", "y", (half - 1, half))
     token_wait(3, block_of(1 - zz, 1 - x, c))
     token(6, block_of(1 - zz, 1 - x, c), sp, core)
     relays("D", "out", "L", 0)
     relays("D", "out", "H", 0)
-    relays("D", "in", "L", 1, 2)
-    relays("D", "in", "H", 1)
+    relays("D", "in", "L", 2)
     detours("D")
     relays("D", "in", "H", 2)
     relays("D", "in", "L", 3)
-    relays("D", "in", "H", 3)
     token_wait(2, block_of(zz, x, 1 - c))
     token_wait(4, block_of(1 - zz, x, 1 - c))
     token_wait(5, block_of(zz, 1 - x, 1 - c))
@@ -854,8 +851,9 @@
         return 0
 
     lax.fori_loop(0, many, ffn_in, 0)
-    middle = sorted(range(ring), key=lambda q: abs(2 * q - ring + 1))
-    order = [(q, 0) for q in middle] + [(q, 1) for q in middle]
+    inner, outer = list(range(half, half - 2, -1)), [q for q in range(ring - 1, -1, -1) if q not in (half - 1, half)]
+    order = [(q, 0) for q in inner + outer[:1]] + [(inner[0], 1)] + [(q, 0) for q in outer[1:]]
+    order += [(q, 1) for q in inner[1:] + outer]
     side = regions["L"][3]
     mids = regions["M"][3] - regions["M"][2]
     base = pl.multiple_of(first * 128, 128)
@@ -912,8 +910,10 @@
         result[:, lanes] = (residual[:, lanes] + ffn).astype(BF16)
 
     ahead = {
-        0: (("out", "L", 2), ("out", "H", 2)),
-        2: (("out", "L", 3), ("out", "H", 3)),
+        0: (("in", "H", 3), ("out", "L", 2)),
+        1: (("out", "H", 2),),
+        2: (("out", "L", 3),),
+        4: (("out", "H", 3),),
     }
     for i in range(n + 5):
         for role, g, step in ahead.get(i, ()):

time: 119 us -> 117 us (0.983)
  Pallas kernels: 117 us -> 115 us
    pallas_call x1, Pallas kernels: 117 us -> 115 us  [paired_body(): pl.pallas_call(functools.partial(paired_kernel, n, tps), out_shape=jax.Sh...]
where the time goes in v4:
time: 117 us; the launch traced here: 116 us
  Pallas kernels  115 us (98%)
  local copies, waits for them, and re-layouts  1.77 us (2%)
    pallas_call x1, Pallas kernels, paired_body(): pl.pallas_call(functools.partial(paired_kernel, n, tps), out_shape=jax.Sh...  115 us

profile of v4, /device:TPU:0, one launch (start us, length us, event | category | flops | bytes accessed | tf_op | source)
XLA Modules:
  0.0 116.4 jit_solution(8597939807475778996)
XLA Ops:
  0.0 114.6 %shard_map.145 = bf16[96,2048]{1,0:T(8,128)(2,1)} custom-call(bf16[96,2048]{1,0:T(8,128)(2,1)} %stream_in.1, bf16[384,256]{1,0:T(8,128)(2,1)} %qp_in.1, bf16[384,256]{1,0:T(8,128)(2,1)} %kp_in.1, bf16[384,256]{1,0:T(8,128)(2,1)} %vp_in.1, bf16[384,256]{1,0:T(8,128)(2,1)} %gp_in.1, bf16[2,384]{1,0:T(2,128)(2,1)} %strength_in.1, bf16[2,384]{1,0:T(2,128)(2,1)} %decay_in.1, ...), custom_call_target="tpu_custom_call" | custom-call | tf_op jit(solution)/shard_map/pallas_call | solution.py:965
  114.6 1.8 %copy.17 = bf16[96,2048]{1,0:T(8,128)(2,1)} copy(bf16[96,2048]{1,0:T(8,128)(2,1)} %shard_map.145) | data formatting | bytes 786432
